TPU v7x, 256 devices: a whole 4x4x8 slice. The times are simulated.
256 devices in a mesh: kv: 16 (over y, x), tp: 16 (over z, core).
Axes of the slice: x: 4, y: 4, z: 8, core: 2. Of those that a mesh axis runs over, the one named last changes fastest.
Arguments:
- tokens: bfloat16 [16, 2048], P(None, 'kv'), may hold values from -40 to 40
- lengths: int32 [16], replicated, may hold values from 1 to 16384, 77824 in all
- cache_keys: bfloat16 [16, 16384, 16, 128], P(None, 'kv', 'tp'), may hold values from -200 to 200
- cache_values: bfloat16 [16, 16384, 16, 128], P(None, 'kv', 'tp'), may hold values from -6 to 6
- lambdas: float32 [16], P('tp'), may hold values from 0.3 to 0.8
- head_gain: bfloat16 [128], replicated, may hold values from 0.099609375 to 1.8984375
- attn_gain: bfloat16 [2048], P('kv'), may hold values from 0.099609375 to 1.8984375
- w_query: bfloat16 [2048, 2048], P('kv', 'tp'), may hold values from -0.125 to 0.125
- w_key: bfloat16 [2048, 2048], P('kv', 'tp'), may hold values from -0.5 to 0.5
- w_value: bfloat16 [2048, 2048], P('kv', 'tp'), may hold values from -0.125 to 0.125
- w_out: bfloat16 [2048, 2048], P('tp', 'kv'), may hold values from -0.125 to 0.125
- first_gain: bfloat16 [2048], P('kv'), may hold values from 0.099609375 to 1.8984375
- first_gate: bfloat16 [2048, 5632], P('kv', 'tp'), may hold values from -0.125 to 0.125
- first_up: bfloat16 [2048, 5632], P('kv', 'tp'), may hold values from -0.125 to 0.125
- first_down: bfloat16 [5632, 2048], P('tp', 'kv'), may hold values from -0.078125 to 0.078125
- second_gain: bfloat16 [2048], P('kv'), may hold values from 0.099609375 to 1.8984375
- second_gate: bfloat16 [2048, 5632], P('kv', 'tp'), may hold values from -0.125 to 0.125
- second_up: bfloat16 [2048, 5632], P('kv', 'tp'), may hold values from -0.125 to 0.125
- second_down: bfloat16 [5632, 2048], P('tp', 'kv'), may hold values from -0.078125 to 0.078125
Outputs:
- stream_out: bfloat16 [16, 2048], P(None, 'kv')
Inputs may be any that keep to these rules, and one draw needn't show every extreme that they name: `lengths`: one sequence has exactly 16384 live positions.
All inputs are finite; a program needn't handle non-finite values.
Results may differ from a plain program's by a relative error of at most 0.02.
Values may be sent and summed in bfloat16 or wider, within the bound.
No kernel may reach another device: no remote copies, remote signals or barrier semaphores. Data moves between devices by JAX's collectives and lax.ppermute only.
A program may use at most 64 MiB of HBM per device.

v0:
```python
import jax
import jax.numpy as jnp
from jax import lax
from jax.sharding import Mesh
from jax.sharding import PartitionSpec as P

D = 2048
DK = 64
DV = 128
KV = ("kv_0", "kv_1")


EPSILON = 1e-06
ROTARY_BASE = 10000.0
OUTPUT_KEEP = 0.8
MASKED_SCORE = -1e30


def one_axis_at_a_time(value, axes):
    for axis in axes:
        value = lax.psum(value, axis)
    return value


def copy_for_each(value, axis):
    copies = jnp.broadcast_to(value, (lax.axis_size(axis), *value.shape))
    return lax.all_to_all(copies, axis, split_axis=0, concat_axis=0, tiled=True)


def taken_together(value, axis):
    everything = copy_for_each(value, axis)
    return jnp.sum(everything, axis=0)


def together(arrays, axis):
    ravelled, at, finished = (jnp.concatenate([a.reshape(-1) for a in arrays]), 0, [])
    running = taken_together(ravelled, axis)
    for a in arrays:
        finished.append(running[at : at + a.size].reshape(a.shape))
        at += a.size
    return tuple(finished)


def all_in_one(value, axis):
    leaves = jax.tree.leaves(value)
    turns = sorted(range(len(leaves)), key=lambda k: -leaves[k].size)
    width = (1, *leaves[turns[0]].shape)[-1]
    lines = [
        jnp.pad(leaves[k].reshape(-1), (0, -leaves[k].size % width)).reshape(-1, width)
        for k in turns
    ]
    both, at, found = (copy_for_each(jnp.concatenate(lines), axis), 0, {})
    for k, line in zip(turns, lines):
        share = both[:, at : at + len(line)].reshape(len(both), -1)
        found[k] = share[:, : leaves[k].size].reshape(-1, *leaves[k].shape)
        at += len(line)
    numbers = iter(range(len(leaves)))
    return jax.tree.map(lambda _: found[next(numbers)], value)


def combined_pairwise(pieces, combine):
    while len(jax.tree.leaves(pieces)[0]) > 1:
        pieces = jax.vmap(combine)(
            *(jax.tree.map(lambda part: part[side::2], pieces) for side in (0, 1))
        )
    return jax.tree.map(lambda part: part[0], pieces)


def combined_all(value, axis, combine):
    pieces = all_in_one(value, axis)
    return combined_pairwise(pieces, combine)


def rotate(vectors, positions):
    half_width = vectors.shape[-1] // 2
    inv_freq = jnp.power(ROTARY_BASE, -jnp.arange(half_width, dtype=jnp.float32) / half_width)
    angles = positions.astype(jnp.float32)[:, None] * inv_freq[None, :]
    bcast_shape = (angles.shape[0],) + (1,) * (vectors.ndim - 2) + (half_width,)
    cosine = jnp.cos(angles).reshape(bcast_shape)
    sine_part = jnp.sin(angles).reshape(bcast_shape)
    first_half = vectors[..., :half_width]
    second_half = vectors[..., half_width:]
    return jnp.concatenate(
        [
            first_half * cosine - second_half * sine_part,
            second_half * cosine + first_half * sine_part,
        ],
        axis=-1,
    )


def channel_mix(stream, gain, w_gate, w_up, w_down):
    stream_f = stream.astype(jnp.float32)
    scaled = (stream_f * gain.astype(jnp.float32)).astype(jnp.bfloat16)
    square = jnp.sum(stream_f * stream_f, axis=1)
    gate_part = jnp.dot(scaled, w_gate, preferred_element_type=jnp.float32)
    up_part = jnp.dot(scaled, w_up, preferred_element_type=jnp.float32)
    square, gate_sum, up_sum = (
        one_axis_at_a_time(square.astype(jnp.bfloat16), KV).astype(jnp.float32),
        one_axis_at_a_time(gate_part.astype(jnp.bfloat16), KV).astype(jnp.float32),
        one_axis_at_a_time(up_part.astype(jnp.bfloat16), KV).astype(jnp.float32),
    )
    row_scale = lax.rsqrt(square / D + EPSILON)[:, None]
    hidden = (jax.nn.silu(row_scale * gate_sum) * (row_scale * up_sum)).astype(jnp.bfloat16)
    partial_value = jnp.dot(hidden, w_down, preferred_element_type=jnp.float32)
    total_sum = taken_together(partial_value, "tp")
    return (stream_f + 0.5 * total_sum).astype(jnp.bfloat16)


def combine_parts(left, right):
    peak_max = jnp.maximum(left[0], right[0])
    left_scale = jnp.exp(left[0] - peak_max)
    right_scale = jnp.exp(right[0] - peak_max)
    return (
        peak_max,
        left[1] * left_scale + right[1] * right_scale,
        left[2] * left_scale[..., None] + right[2] * right_scale[..., None],
    )


def token_mix(
    stream,
    lengths,
    cache_keys,
    cache_values,
    lambdas,
    head_gain,
    attn_gain,
    w_query,
    w_key,
    w_value,
    w_out,
):
    seq_count = stream.shape[0]
    heads_dev = lambdas.shape[0]
    pos_count = cache_keys.shape[1]
    scale_att = DK ** (-0.5)
    stream_f = stream.astype(jnp.float32)
    scaled = (stream_f * attn_gain.astype(jnp.float32)).astype(jnp.bfloat16)
    square = jnp.sum(stream_f * stream_f, axis=1)
    query_part = jnp.dot(scaled, w_query, preferred_element_type=jnp.float32)
    key_part = jnp.dot(scaled, w_key, preferred_element_type=jnp.float32)
    value_part = jnp.dot(scaled, w_value, preferred_element_type=jnp.float32)
    square, query_sum, key_sum, value_sum = together((square, query_part, key_part, value_part), KV)
    row_scale = lax.rsqrt(square / D + EPSILON)[:, None]
    query = rotate((row_scale * query_sum).reshape(seq_count, heads_dev, 2, DK), lengths).astype(
        jnp.bfloat16
    )
    key_new = rotate((row_scale * key_sum).reshape(seq_count, heads_dev, 2, DK), lengths).astype(
        jnp.bfloat16
    )
    value_new = (row_scale * value_sum).astype(jnp.bfloat16).reshape(seq_count, heads_dev, DV)
    key_rows = cache_keys.reshape(seq_count, pos_count, heads_dev, 2, DK)
    scores = (
        jnp.einsum("bhcd,bphcd->bhcp", query, key_rows, preferred_element_type=jnp.float32)
        * scale_att
    )
    places = lax.axis_index(KV) * pos_count + jnp.arange(pos_count, dtype=jnp.int32)
    live_mask = (places[None, :] < lengths[:, None])[:, None, None, :]
    scores = jnp.where(live_mask, scores, MASKED_SCORE)
    block_max = jnp.max(scores, axis=3)
    weights = jnp.where(live_mask, jnp.exp(scores - block_max[..., None]), 0.0)
    total_sum = jnp.sum(weights, axis=3)
    values = jnp.einsum(
        "bhcp,bphd->bhcd",
        weights.astype(jnp.bfloat16),
        cache_values,
        preferred_element_type=jnp.float32,
    )
    block_max, total_sum, values = combined_all((block_max, total_sum, values), KV, combine_parts)
    own_score = jnp.sum(query.astype(jnp.float32) * key_new.astype(jnp.float32), axis=3) * scale_att
    peak_max = jnp.maximum(block_max, own_score)
    old_scale = jnp.exp(block_max - peak_max)
    fresh_weight = jnp.exp(own_score - peak_max)
    denominator = total_sum * old_scale + fresh_weight
    mixed = (
        values * old_scale[..., None]
        + fresh_weight[..., None] * value_new.astype(jnp.float32)[:, :, None, :]
    ) / denominator[..., None]
    heads_out = mixed[:, :, 0] - lambdas[None, :, None] * mixed[:, :, 1]
    norm_scale = lax.rsqrt(jnp.mean(heads_out * heads_out, axis=2, keepdims=True) + EPSILON)
    normed = (heads_out * norm_scale * head_gain.astype(jnp.float32) * OUTPUT_KEEP).astype(
        jnp.bfloat16
    )
    normed = normed.reshape(seq_count, heads_dev * DV)
    partial_value = jnp.dot(normed, w_out, preferred_element_type=jnp.float32)
    projected = taken_together(partial_value, "tp")
    return (stream_f + projected).astype(jnp.bfloat16)


def local(
    tokens,
    lengths,
    cache_keys,
    cache_values,
    lambdas,
    head_gain,
    attn_gain,
    w_query,
    w_key,
    w_value,
    w_out,
    first_gain,
    first_gate,
    first_up,
    first_down,
    second_gain,
    second_gate,
    second_up,
    second_down,
):
    first = channel_mix(tokens, first_gain, first_gate, first_up, first_down)
    second = token_mix(
        first,
        lengths,
        cache_keys,
        cache_values,
        lambdas,
        head_gain,
        attn_gain,
        w_query,
        w_key,
        w_value,
        w_out,
    )
    return channel_mix(second, second_gain, second_gate, second_up, second_down)


def solution(mesh):
    finer = Mesh(mesh.devices.reshape(4, 4, mesh.shape["tp"]), ("kv_0", "kv_1", "tp"))
    placed = (
        P(None, KV),
        P(),
        P(None, KV, "tp", None),
        P(None, KV, "tp", None),
        P("tp"),
        P(),
        P(KV),
        P(KV, "tp"),
        P(KV, "tp"),
        P(KV, "tp"),
        P("tp", KV),
        P(KV),
        P(KV, "tp"),
        P(KV, "tp"),
        P("tp", KV),
        P(KV),
        P(KV, "tp"),
        P(KV, "tp"),
        P("tp", KV),
    )
    return jax.shard_map(local, mesh=finer, in_specs=placed, out_specs=P(None, KV), check_vma=False)
```

profile of v0, /device:TPU:1, one launch (start us, length us, event | category | flops | bytes accessed | tf_op | source)
XLA Modules:
  0.0 159.8 jit_solution(13834522960345422851)
XLA Ops:
  0.0 0.7 convert_element_type.160
  0.7 0.8 fusion.16
  1.5 0.8 convolution_convert_fusion.2
  2.3 1.1 convolution_convert_fusion.3
  3.4 14.4 %all-reduce.5 = (bf16[16,352]{1,0:T(8,128)(2,1)S(1)}, bf16[16,352]{1,0:T(8,128)(2,1)S(1)}, bf16[16]{0:T(256)(128)(2,1)S(1)}) all-reduce(bf16[16,352]{1,0:T(8,128)(2,1)S(1)} %convolution_convert_fusion.2, bf16[16,352]{1,0:T(8,128)(2,1)S(1)} %convolution_convert_fusion.3, ...), channel_id=1, replica_groups=mesh['kv_0'=4,'kv_1'=4,'tp'=16] {'kv_0'}, use_global_device_ids=true, to_apply=%region_5.0 | all-reduce | flops 11280 | bytes 45120 | tf_op jit(solution)/shard_map/psum | solution.py:21
  17.8 13.3 %all-reduce.3 = (bf16[16,352]{1,0:T(8,128)(2,1)S(1)}, bf16[16,352]{1,0:T(8,128)(2,1)S(1)}, bf16[16]{0:T(256)(128)(2,1)S(1)}) all-reduce(bf16[16,352]{1,0:T(8,128)(2,1)S(1)} %get-tuple-element.14, bf16[16,352]{1,0:T(8,128)(2,1)S(1)} %get-tuple-element.15, ...), channel_id=1, replica_groups=mesh['kv_0'=4,'kv_1'=4,'tp'=16] {'kv_1'}, use_global_device_ids=true, to_apply=%region_6.0 | all-reduce | flops 11280 | bytes 45120 | tf_op jit(solution)/shard_map/psum | solution.py:21
  31.1 1.1 fusion.10
  32.2 0.7 broadcast_in_dim.28
  32.8 16.7 %all-to-all-start = ((f32[16,16,128]{2,1,0:T(8,128)}), f32[16,16,128]{2,1,0:T(8,128)S(1)}, u32[]{:S(2)}, u32[]{:S(2)}) async-start(f32[16,16,128]{2,1,0:T(8,128)} %broadcast_in_dim.28), calls=%async_computation | async-start | bytes 262144 | tf_op jit(solution)/shard_map/all_to_all | solution.py:27
  49.5 0.7 convert_element_type.169
  50.2 0.7 convert_element_type.171
  50.8 7.6 %all-to-all-done = f32[16,16,128]{2,1,0:T(8,128)S(1)} async-done(((f32[16,16,128]{2,1,0:T(8,128)}), f32[16,16,128]{2,1,0:T(8,128)S(1)}, u32[]{:S(2)}, u32[]{:S(2)}) %all-to-all-start) | async-done | bytes 131104 | tf_op jit(solution)/shard_map/all_to_all | solution.py:27
  58.4 0.8 fusion.19
  59.2 0.9 convolution_bitcast_fusion
  60.1 0.9 convolution_bitcast_fusion.2
  61.0 0.9 convolution_bitcast_fusion.1
  62.0 1.0 broadcast_in_dim.30
  62.9 3.6 %all-to-all-start.1 = ((f32[16,1,6160]{2,1,0:T(1,128)}), f32[16,1,6160]{2,1,0:T(1,128)S(1)}, u32[]{:S(2)}, u32[]{:S(2)}) async-start(f32[16,1,6160]{2,1,0:T(1,128)} %broadcast_in_dim.30), calls=%async_computation.1 | async-start | bytes 802816 | tf_op jit(solution)/shard_map/all_to_all | solution.py:27
  66.5 0.1 multiply_cosine_fusion
  66.6 6.4 %copy.202 = bf16[16,1024,1,128]{1,3,0,2:T(8,128)(2,1)} copy(bf16[16,1024,1,128]{3,1,2,0:T(8,128)(2,1)} %param.21) | data formatting | bytes 8388608 | tf_op args[2]
  73.1 3.3 %all-to-all-done.1 = f32[16,1,6160]{2,1,0:T(1,128)S(1)} async-done(((f32[16,1,6160]{2,1,0:T(1,128)}), f32[16,1,6160]{2,1,0:T(1,128)S(1)}, u32[]{:S(2)}, u32[]{:S(2)}) %all-to-all-start.1) | async-done | bytes 394272 | tf_op jit(solution)/shard_map/all_to_all | solution.py:27
  76.4 0.3 reduce_sum.93
  77.2 2.9 %fusion.8 = f32[16,2,1,1024]{3,2,1,0:T(1,128)S(1)} fusion(bf16[16,1024,2,64]{1,3,2,0:T(8,128)(2,1)} %bitcast.96, bf16[16,2,64,1]{2,0,1,3:T(8,128)(2,1)S(1)} %maximum_bitcast_fusion), kind=kOutput, calls=%fused_computation.27 | convolution fusion | flops 4194304 | bytes 4329472 | tf_op jit(solution)/shard_map/bhcd,bphcd->bhcp/dot_general | solution.py:155
  80.0 0.2 fusion.4
  80.3 0.3 fusion.59
  80.7 3.0 %fusion = f32[16,2,128]{2,1,0:T(2,128)S(1)} fusion(bf16[16,1024,1,128]{3,1,2,0:T(8,128)(2,1)} %param.22, pred[16,1024]{1,0:T(8,128)(4,1)S(1)} %broadcast_compare_fusion, f32[16,2]{1,0:T(8,128)S(1)} %fusion.4, f32[16,2,1,1024]{3,2,1,0:T(1,128)S(1)} %fusion.8), kind=kOutput, calls=%fused_computation | convolution fusion | flops 8552448 | bytes 4358272 | tf_op jit(solution)/shard_map/bhcp,bphd->bhcd/dot_general | solution.py:164
  83.7 0.1 reshape.496
  83.8 0.7 broadcast_in_dim.33
  84.5 3.5 %all-to-all-start.2 = ((f32[16,34,128]{2,1,0:T(8,128)}), f32[16,34,128]{2,1,0:T(8,128)S(1)}, u32[]{:S(2)}, u32[]{:S(2)}) async-start(f32[16,34,128]{2,1,0:T(8,128)} %broadcast_in_dim.33), calls=%async_computation.2 | async-start | bytes 655360 | tf_op jit(solution)/shard_map/all_to_all | solution.py:27
  88.7 0.2 multiply_reduce_fusion
  89.0 7.3 %all-to-all-done.2 = f32[16,34,128]{2,1,0:T(8,128)S(1)} async-done(((f32[16,34,128]{2,1,0:T(8,128)}), f32[16,34,128]{2,1,0:T(8,128)S(1)}, u32[]{:S(2)}, u32[]{:S(2)}) %all-to-all-start.2) | async-done | bytes 278560 | tf_op jit(solution)/shard_map/all_to_all | solution.py:27
  96.3 0.1 copy.237
  96.4 0.1 slice.152
  96.5 0.1 slice.153
  96.7 0.1 copy.232
  96.8 0.1 slice.131
  96.9 0.1 slice.132
  97.6 0.2 copy.231
  97.8 0.3 slice.133
  98.1 0.3 slice.128
  98.5 0.1 multiply_add_fusion
  98.7 0.4 slice.137
  99.0 0.4 slice.134
  99.4 0.1 copy.209
  99.5 0.1 copy.210
  99.6 0.1 multiply_add_fusion.1
  99.8 0.3 slice.141
  100.1 0.3 slice.138
  100.7 0.1 copy.212
  100.9 0.1 multiply_add_fusion.2
  101.0 0.1 fusion.5
  101.2 0.1 multiply_reduce_fusion.1
  101.4 0.2 fusion.31
  101.6 0.7 broadcast_in_dim.34
  102.2 5.4 %all-to-all-start.3 = ((f32[16,16,128]{2,1,0:T(8,128)}), f32[16,16,128]{2,1,0:T(8,128)S(1)}, u32[]{:S(2)}, u32[]{:S(2)}) async-start(f32[16,16,128]{2,1,0:T(8,128)} %broadcast_in_dim.34), calls=%async_computation.3 | async-start | bytes 262144 | tf_op jit(solution)/shard_map/all_to_all | solution.py:27
  107.6 9.2 %all-to-all-done.3 = f32[16,16,128]{2,1,0:T(8,128)S(1)} async-done(((f32[16,16,128]{2,1,0:T(8,128)}), f32[16,16,128]{2,1,0:T(8,128)S(1)}, u32[]{:S(2)}, u32[]{:S(2)}) %all-to-all-start.3) | async-done | bytes 131104 | tf_op jit(solution)/shard_map/all_to_all | solution.py:27
  116.8 0.1 fusion.22
  116.9 0.1 convolution_convert_fusion.1
  117.1 0.1 convolution_convert_fusion
  117.2 11.4 %all-reduce.4 = (bf16[16,352]{1,0:T(8,128)(2,1)S(1)}, bf16[16,352]{1,0:T(8,128)(2,1)S(1)}, bf16[16]{0:T(256)(128)(2,1)S(1)}) all-reduce(bf16[16,352]{1,0:T(8,128)(2,1)S(1)} %convolution_convert_fusion, bf16[16,352]{1,0:T(8,128)(2,1)S(1)} %convolution_convert_fusion.1, ...), channel_id=1, replica_groups=mesh['kv_0'=4,'kv_1'=4,'tp'=16] {'kv_0'}, use_global_device_ids=true, to_apply=%region_20.21 | all-reduce | flops 11280 | bytes 45120 | tf_op jit(solution)/shard_map/psum | solution.py:21
  128.6 11.9 %all-reduce.2 = (bf16[16,352]{1,0:T(8,128)(2,1)S(1)}, bf16[16,352]{1,0:T(8,128)(2,1)S(1)}, bf16[16]{0:T(256)(128)(2,1)S(1)}) all-reduce(bf16[16,352]{1,0:T(8,128)(2,1)S(1)} %get-tuple-element.11, bf16[16,352]{1,0:T(8,128)(2,1)S(1)} %get-tuple-element.12, ...), channel_id=1, replica_groups=mesh['kv_0'=4,'kv_1'=4,'tp'=16] {'kv_1'}, use_global_device_ids=true, to_apply=%region_21.22 | all-reduce | flops 11280 | bytes 45120 | tf_op jit(solution)/shard_map/psum | solution.py:21
  140.5 0.2 fusion.11
  140.7 18.5 %all_to_all.26 = f32[16,16,128]{2,1,0:T(8,128)S(1)} all-to-all(f32[16,16,128]{2,1,0:T(8,128)S(1)} %broadcast_in_dim.35), channel_id=1, replica_groups=mesh['kv_0'=4,'kv_1'=4,'tp'=16] {'tp'}, dimensions={0} | all-to-all | bytes 262144 | tf_op jit(solution)/shard_map/all_to_all | solution.py:27
  159.2 0.6 fusion.24
  (70 shorter events, 2.1 us)
Async XLA Ops:
  0.0 1.5 copy-start
  32.8 25.6 %all-to-all-start = ((f32[16,16,128]{2,1,0:T(8,128)}), f32[16,16,128]{2,1,0:T(8,128)S(1)}, u32[]{:S(2)}, u32[]{:S(2)}) async-start(f32[16,16,128]{2,1,0:T(8,128)} %broadcast_in_dim.28), calls=%async_computation | async-start | bytes 262144 | tf_op jit(solution)/shard_map/all_to_all | solution.py:27
  62.9 13.5 %all-to-all-start.1 = ((f32[16,1,6160]{2,1,0:T(1,128)}), f32[16,1,6160]{2,1,0:T(1,128)S(1)}, u32[]{:S(2)}, u32[]{:S(2)}) async-start(f32[16,1,6160]{2,1,0:T(1,128)} %broadcast_in_dim.30), calls=%async_computation.1 | async-start | bytes 802816 | tf_op jit(solution)/shard_map/all_to_all | solution.py:27
  66.6 6.4 %copy-start.3 = (s32[16]{0:T(128)S(1)}, s32[16]{0:T(128)}, u32[]{:S(2)}) copy-start(s32[16]{0:T(128)} %param.20) | copy-start | bytes 196
  77.2 11.5 %copy-start.6 = (bf16[128]{0:T(256)(128)(2,1)S(1)}, bf16[128]{0:T(256)(128)(2,1)}, u32[]{:S(2)}) copy-start(bf16[128]{0:T(256)(128)(2,1)} %param.24) | copy-start | bytes 772
  80.6 20.7 %copy-start.5 = (bf16[128,128]{1,0:T(8,128)(2,1)S(1)}, bf16[128,128]{1,0:T(8,128)(2,1)}, u32[]{:S(2)}) copy-start(bf16[128,128]{1,0:T(8,128)(2,1)} %param.29) | copy-start | bytes 98308
  80.6 26.9 %copy-start.7 = (bf16[128]{0:T(256)(128)(2,1)S(1)}, bf16[128]{0:T(256)(128)(2,1)}, u32[]{:S(2)}) copy-start(bf16[128]{0:T(256)(128)(2,1)} %param.34) | copy-start | bytes 772
  80.7 36.3 %copy-start.1 = (bf16[128,352]{0,1:T(8,128)(2,1)S(1)}, bf16[128,352]{0,1:T(8,128)(2,1)}, u32[]{:S(2)}) copy-start(bf16[128,352]{0,1:T(8,128)(2,1)} %param.35) | copy-start | bytes 270340
  80.7 36.4 %copy-start.2 = (bf16[128,352]{0,1:T(8,128)(2,1)S(1)}, bf16[128,352]{0,1:T(8,128)(2,1)}, u32[]{:S(2)}) copy-start(bf16[128,352]{0,1:T(8,128)(2,1)} %param.36) | copy-start | bytes 270340
  80.7 59.8 %copy-start.4 = (bf16[352,128]{1,0:T(8,128)(2,1)S(1)}, bf16[352,128]{1,0:T(8,128)(2,1)}, u32[]{:S(2)}) copy-start(bf16[352,128]{1,0:T(8,128)(2,1)} %param.37) | copy-start | bytes 270340
  84.5 11.8 %all-to-all-start.2 = ((f32[16,34,128]{2,1,0:T(8,128)}), f32[16,34,128]{2,1,0:T(8,128)S(1)}, u32[]{:S(2)}, u32[]{:S(2)}) async-start(f32[16,34,128]{2,1,0:T(8,128)} %broadcast_in_dim.33), calls=%async_computation.2 | async-start | bytes 655360 | tf_op jit(solution)/shard_map/all_to_all | solution.py:27
  102.2 14.6 %all-to-all-start.3 = ((f32[16,16,128]{2,1,0:T(8,128)}), f32[16,16,128]{2,1,0:T(8,128)S(1)}, u32[]{:S(2)}, u32[]{:S(2)}) async-start(f32[16,16,128]{2,1,0:T(8,128)} %broadcast_in_dim.34), calls=%async_computation.3 | async-start | bytes 262144 | tf_op jit(solution)/shard_map/all_to_all | solution.py:27
where the time goes:
time: 161 us; the launch traced here: 160 us
  blocking collectives  69.4 us (43%)
  starting transfers between devices  29.1 us (18%)
  waiting for transfers between devices  27.3 us (17%)
  local copies, waits for them, and re-layouts  14 us (9%)
  matrix products  12.1 us (8%)
  other arithmetic  6.69 us (4%)
    psum x4, blocking collectives, one_axis_at_a_time(): value = lax.psum(value, axis)  51 us
    all_to_all x4, starting transfers between devices, copy_for_each(): return lax.all_to_all(copies, axis, split_axis=0, concat_axis=0, tiled=True)  29.1 us
    all_to_all x4, waiting for transfers between devices, copy_for_each(): return lax.all_to_all(copies, axis, split_axis=0, concat_axis=0, tiled=True)  27.3 us
    all_to_all x1, blocking collectives, copy_for_each(): return lax.all_to_all(copies, axis, split_axis=0, concat_axis=0, tiled=True)  18.5 us
    unnamed x24, local copies, waits for them, and re-layouts  7.09 us
  transfers between devices with their start and end apart: 4, of which 4 were waited for; matrix products, arithmetic and copies ran while one was open for 5% of the time, Pallas kernels for 0%

commit v1 on v0

v1 whole, which is shorter than its diff:
```python
import functools
import math

import jax
import jax.numpy as jnp
from jax import lax
from jax.experimental import pallas as pl
from jax.experimental.pallas import tpu as pltpu
from jax.sharding import Mesh
from jax.sharding import PartitionSpec as P

D = 2048
DK = 64
DV = 128
SEQS = 16
KV = ("kv_0", "kv_1")
EPSILON = 1e-06
ROTARY_BASE = 10000.0
OUTPUT_KEEP = 0.8
MASKED_SCORE = -1e30
F32 = jnp.float32
BF16 = jnp.bfloat16


def exchange(copies, axis):
    return lax.all_to_all(copies, axis, split_axis=0, concat_axis=0, tiled=True)


def cost(micros):
    return pl.CostEstimate(flops=int(micros * 5e8), bytes_accessed=1 << 16, transcendentals=0)


def local_call(body, outs, *arrays, scratch=(), smem=()):
    specs = [
        pl.BlockSpec(memory_space=pltpu.SMEM if i in smem else pltpu.VMEM)
        for i in range(len(arrays))
    ]
    return pl.pallas_call(
        body,
        out_shape=outs,
        in_specs=specs,
        out_specs=jax.tree.map(lambda _: pl.BlockSpec(memory_space=pltpu.VMEM), outs),
        scratch_shapes=list(scratch),
        compiler_params=pltpu.CompilerParams(vmem_limit_bytes=4 << 20),
        cost_estimate=cost(10),
    )(*arrays)


def dot_rows(a, b):
    return lax.dot_general(a, b, (((1,), (1,)), ((), ())), preferred_element_type=F32)


def dot(a, b):
    return jnp.dot(a, b, preferred_element_type=F32)


def put_copies(out_ref, at, value):
    for j in range(out_ref.shape[0]):
        out_ref[j, :, at : at + value.shape[1]] = value


def pieces(value, count):
    parts = []
    for _ in range(count):
        part = value.astype(BF16)
        parts.append(part)
        value = value - part.astype(F32)
    return parts


def with_columns(width, columns):
    lane = lax.broadcasted_iota(jnp.int32, (columns[0].shape[0], width), 1)
    out = jnp.zeros(lane.shape, F32)
    for i, c in enumerate(columns):
        out = jnp.where(lane == i, c.astype(F32), out)
    return out.astype(BF16)


def total(ref):
    out = ref[0].astype(F32)
    for j in range(1, ref.shape[0]):
        out = out + ref[j].astype(F32)
    return out


def gate_up_products(stream_f, gain_ref, gate_ref, up_ref, out_ref):
    scaled = (stream_f * gain_ref[...].astype(F32)).astype(BF16)
    square = jnp.sum(stream_f * stream_f, axis=1, keepdims=True)
    gate = dot_rows(scaled, gate_ref[...]).astype(BF16)
    up = dot_rows(scaled, up_ref[...]).astype(BF16)
    put_copies(out_ref, 0, gate)
    put_copies(out_ref, 352, with_columns(32, pieces(square, 2)))
    put_copies(out_ref, 384, up)
    put_copies(out_ref, 736, jnp.zeros((SEQS, 32), BF16))


def first_products(
    tokens_ref, gain_ref, gate_ref, up_ref, lambda_ref, out_ref, lambda_out, tokens, gain, gate, up,
    lam, sems
):
    copies = [
        pltpu.make_async_copy(src, dst, sems.at[i])
        for i, (src, dst) in enumerate(
            (
                (gate_ref, gate), (up_ref, up), (tokens_ref, tokens), (gain_ref, gain),
                (lambda_ref, lam),
            )
        )
    ]
    for copy in copies:
        copy.start()
    for copy in copies:
        copy.wait()
    gate_up_products(tokens[...].astype(F32), gain, gate, up, out_ref)
    lambda_out[...] = jnp.full(lambda_out.shape, lam[0], F32)


def second_products(stream_ref, got_ref, gain_ref, gate_ref, up_ref, out_ref, second_ref):
    second = (stream_ref[...].astype(F32) + total(got_ref)).astype(BF16)
    second_ref[...] = second
    gate_up_products(second.astype(F32), gain_ref, gate_ref, up_ref, out_ref)


def down_products(got_ref, down_ref, out_ref):
    summed = total(got_ref)
    square = summed[:, 352:353] + summed[:, 353:354]
    row_scale = lax.rsqrt(square / D + EPSILON)
    gate = row_scale * summed[:, :352]
    up = row_scale * summed[:, 384:736]
    hidden = (gate / (1.0 + jnp.exp(-gate)) * up).astype(BF16)
    put_copies(out_ref, 0, dot(hidden, down_ref[...]).astype(BF16))


def head_products(tokens_ref, got_ref, gain_ref, wq_ref, wk_ref, wv_ref, out_ref, first_ref):
    first = (tokens_ref[...].astype(F32) + 0.5 * total(got_ref)).astype(BF16)
    first_ref[...] = first
    stream_f = first.astype(F32)
    scaled = (stream_f * gain_ref[...].astype(F32)).astype(BF16)
    square = jnp.sum(stream_f * stream_f, axis=1, keepdims=True)
    query = dot(scaled, wq_ref[...]).astype(BF16)
    key = dot(scaled, wk_ref[...])
    value = dot(scaled, wv_ref[...])
    diagonal = lax.broadcasted_iota(jnp.int32, (SEQS, 128), 0) == lax.broadcasted_iota(
        jnp.int32, (SEQS, 128), 1
    )
    high, rest = pieces(jnp.sum(jnp.where(diagonal, square, 0.0), axis=0, keepdims=True), 2)
    row = lax.broadcasted_iota(jnp.int32, (8, 128), 0)
    squares = jnp.where(row == 2, high.astype(F32), jnp.where(row == 3, rest.astype(F32), 0.0))
    for j in range(SEQS):
        out_ref[j, :SEQS, :] = query
        tail = jnp.where(row == 0, key[j : j + 1], jnp.where(row == 1, value[j : j + 1], squares))
        out_ref[j, SEQS:, :] = tail.astype(BF16)


def rotary_tables(lengths_ref, rows, width):
    lane = lax.broadcasted_iota(jnp.int32, (rows, width), 1)
    row = lax.broadcasted_iota(jnp.int32, (rows, width), 0)
    place = jnp.zeros((rows, width), jnp.int32)
    for b in range(rows):
        place = jnp.where(row == b, lengths_ref[b], place)
    half = DK // 2
    step = (lane % half).astype(F32)
    angles = place.astype(F32) * jnp.exp(step * (-math.log(ROTARY_BASE) / half))
    low = (lane // half) % 2 == 0
    sine = jnp.sin(angles)
    return jnp.cos(angles), jnp.where(low, -sine, sine), low, lane


def attention(lengths_ref, got_ref, keys_ref, values_ref, out_ref):
    summed = total(got_ref)
    cosine, sine, low, lane = rotary_tables(lengths_ref, SEQS, 2 * DK)
    row = lax.broadcasted_iota(jnp.int32, lane.shape, 0)
    kv_index = lax.axis_index(KV)
    mine = row == kv_index
    square = jnp.sum(
        jnp.where(row == lane, summed[18:19] + summed[19:20], 0.0), axis=1, keepdims=True
    )
    row_scale = lax.rsqrt(square / D + EPSILON)

    def of_mine(x):
        return jnp.sum(jnp.where(mine, x, 0.0), axis=0, keepdims=True)

    def rotate(x, cosine, sine, low):
        swapped = jnp.where(low, pltpu.roll(x, 96, 1), pltpu.roll(x, 32, 1))
        return (x * cosine + swapped * sine).astype(BF16).astype(F32)

    def eight(x):
        return jnp.broadcast_to(x, (8, x.shape[1]))

    query = rotate(row_scale * summed[:SEQS], cosine, sine, low)
    my_scale = of_mine(jnp.broadcast_to(row_scale, lane.shape))
    key_new = rotate(
        eight(my_scale * summed[16:17]), eight(of_mine(cosine)), eight(of_mine(sine)), low[:8]
    )[:1]
    value_new = (my_scale * summed[17:18]).astype(BF16).astype(F32)
    scale_att = DK ** (-0.5)
    first_part = lane < DK
    both = jnp.concatenate(
        [jnp.where(first_part, query, 0.0), jnp.where(first_part, 0.0, query)], axis=0
    )
    rows = 2 * SEQS
    positions = keys_ref.shape[1]
    of_row = lax.broadcasted_iota(jnp.int32, (rows, DV), 0) % SEQS
    limit = jnp.zeros((rows, 1), jnp.int32)
    s = jnp.zeros((rows, positions), F32)
    for b in range(SEQS):
        picked = jnp.where(of_row == b, both, 0.0).astype(BF16)
        s = s + dot_rows(picked, keys_ref[b])
        limit = jnp.where(of_row[:, :1] == b, lengths_ref[b] - kv_index * positions, limit)
    alive = lax.broadcasted_iota(jnp.int32, (rows, positions), 1) < limit
    s = jnp.where(alive, s * scale_att, MASKED_SCORE)
    old = jnp.max(s, axis=1, keepdims=True)
    e = jnp.where(alive, jnp.exp(s - old), 0.0)
    l = jnp.sum(e, axis=1, keepdims=True)
    weights = e.astype(BF16)
    o = jnp.zeros((rows, DV), F32)
    for b in range(SEQS):
        o = jnp.where(of_row == b, dot(weights, values_ref[b]), o)
    here = of_row[:, :1] == kv_index
    own_score = scale_att * jnp.sum(both * key_new, axis=1, keepdims=True)
    own_score = jnp.where(here, own_score, MASKED_SCORE)
    peak = jnp.maximum(old, own_score)
    old_scale = jnp.exp(old - peak)
    fresh = jnp.where(here, jnp.exp(own_score - peak), 0.0)
    l = l * old_scale + fresh
    o = (o * old_scale + fresh * value_new).astype(BF16)
    lane = lane[:8]
    stats = jnp.zeros((8, DV), F32)
    for at, part in zip((0, 32, 64, 96, 112), pieces(peak, 3) + pieces(l, 2)):
        for g in range(4):
            stats = jnp.where(lane == at + g, part[8 * g : 8 * g + 8].astype(F32), stats)
    stats = stats.astype(BF16)
    for j in range(out_ref.shape[0]):
        out_ref[j, :rows, :] = o
        out_ref[j, rows:, :] = stats


def out_products(got_ref, lambda_ref, gain_ref, w_ref, out_ref):
    count = got_ref.shape[0]
    rows = 2 * SEQS
    stats = [got_ref[j, rows:, :].astype(F32) for j in range(count)]
    peaks = [x + pltpu.roll(x, 96, 1) + pltpu.roll(x, 64, 1) for x in stats]
    sums = [pltpu.roll(x, 32, 1) + pltpu.roll(x, 16, 1) for x in stats]
    peak = functools.reduce(jnp.maximum, peaks)
    scales = [jnp.exp(p - peak) for p in peaks]
    inverse = 1.0 / sum(w * l for w, l in zip(scales, sums))
    mixed = []
    for g in range(4):
        part = sum(
            w[:, g : g + 1] * got_ref[j, 8 * g : 8 * g + 8, :].astype(F32)
            for j, w in enumerate(scales)
        )
        mixed.append(part * inverse[:, g : g + 1])
    head = jnp.concatenate(mixed[:2], axis=0) - lambda_ref[:1] * jnp.concatenate(mixed[2:], axis=0)
    norm_scale = lax.rsqrt(jnp.mean(head * head, axis=1, keepdims=True) + EPSILON)
    normed = (head * norm_scale * gain_ref[...].astype(F32) * OUTPUT_KEEP).astype(BF16)
    put_copies(out_ref, 0, dot(normed, w_ref[...]).astype(BF16))


def last_sum(stream_ref, got_ref, out_ref):
    out_ref[...] = (stream_ref[...].astype(F32) + 0.5 * total(got_ref)).astype(BF16)


def local(
    tokens, lengths, cache_keys, cache_values, lambdas, head_gain, attn_gain, w_query, w_key,
    w_value, w_out, first_gain, first_gate, first_up, first_down, second_gain, second_gate,
    second_up, second_down,
):
    keys = cache_keys.reshape(SEQS, -1, 2 * DK)
    values = cache_values.reshape(SEQS, -1, DV)
    row = lambda g: g.reshape(1, -1)
    shape = jax.ShapeDtypeStruct
    wide = shape((16, SEQS, 768), BF16)
    narrow = shape((16, SEQS, 128), BF16)
    stream = shape((SEQS, 128), BF16)

    sent, lam = pl.pallas_call(
        first_products,
        out_shape=(wide, shape((8, 128), F32)),
        in_specs=[pl.BlockSpec(memory_space=pltpu.HBM)] * 5,
        out_specs=[pl.BlockSpec(memory_space=pltpu.VMEM)] * 2,
        scratch_shapes=[
            pltpu.VMEM((SEQS, 128), BF16), pltpu.VMEM((1, 128), BF16),
            pltpu.VMEM((352, 128), BF16), pltpu.VMEM((352, 128), BF16),
            pltpu.SMEM((1,), F32), pltpu.SemaphoreType.DMA((5,)),
        ],
        compiler_params=pltpu.CompilerParams(vmem_limit_bytes=60 << 20),
        cost_estimate=cost(10),
    )(tokens, row(first_gain), first_gate.T, first_up.T, lambdas)
    sent = local_call(down_products, narrow, exchange(sent, KV), first_down)
    sent, first = local_call(
        head_products, (shape((16, SEQS + 8, 128), BF16), stream),
        tokens, exchange(sent, "tp"), row(attn_gain), w_query, w_key, w_value,
    )
    sent = local_call(
        attention, shape((16, 2 * SEQS + 8, 128), BF16),
        lengths, exchange(sent, KV), keys, values, smem=(0,),
    )
    sent = local_call(
        out_products, narrow, exchange(sent, KV), lam, row(head_gain), w_out
    )
    sent, second = local_call(
        second_products, (wide, stream),
        first, exchange(sent, "tp"), row(second_gain), second_gate.T, second_up.T,
    )
    sent = local_call(down_products, narrow, exchange(sent, KV), second_down)
    return local_call(last_sum, stream, second, exchange(sent, "tp"))


def solution(mesh):
    finer = Mesh(mesh.devices.reshape(4, 4, mesh.shape["tp"]), ("kv_0", "kv_1", "tp"))
    cache = P(None, KV, "tp", None)
    placed = (
        P(None, KV), P(), cache, cache, P("tp"), P(), P(KV), P(KV, "tp"), P(KV, "tp"),
        P(KV, "tp"), P("tp", KV), P(KV), P(KV, "tp"), P(KV, "tp"), P("tp", KV), P(KV),
        P(KV, "tp"), P(KV, "tp"), P("tp", KV),
    )
    return jax.shard_map(local, mesh=finer, in_specs=placed, out_specs=P(None, KV), check_vma=False)
```

time: 161 us -> 99.6 us (0.62)
  starting transfers between devices: 29.1 us -> 0 us
  waiting for transfers between devices: 27.3 us -> 0 us
  blocking collectives: 69.4 us -> 91.3 us
  local copies, waits for them, and re-layouts: 14 us -> 0.09 us
  matrix products: 12.1 us -> 0 us
  Pallas kernels: 0 us -> 6.97 us
  other arithmetic: 6.69 us -> 0 us
    all_to_all x1 -> x7, blocking collectives: 18.5 us -> 91.3 us  [exchange(): return lax.all_to_all(copies, axis, split_axis=0, concat_axis=0, tiled=True)]
    psum x4 -> x0, blocking collectives: 51 us -> none  [one_axis_at_a_time(): value = lax.psum(value, axis)]
    all_to_all x4 -> x0, starting transfers between devices: 29.1 us -> none  [copy_for_each(): return lax.all_to_all(copies, axis, split_axis=0, concat_axis=0, tiled=True)]
    all_to_all x4 -> x0, waiting for transfers between devices: 27.3 us -> none  [copy_for_each(): return lax.all_to_all(copies, axis, split_axis=0, concat_axis=0, tiled=True)]
    dot_general x12 -> x0, matrix products: 12.1 us -> none  [the longest x1 2.98 us: token_mix(): jnp.einsum('bhcp,bphd->bhcd', weights.astype(jnp.bfloat16), cache_values,...]
    unnamed x24 -> x32, local copies, waits for them, and re-layouts: 7.09 us -> 0.09 us
    pallas_call x0 -> x8, Pallas kernels: none -> 6.97 us  [the longest x7 4.99 us: local_call(): pl.pallas_call(body, out_shape=outs, in_specs=specs, out_specs=jax.tree.m...]
    broadcast_in_dim x5 -> x0, local copies, waits for them, and re-layouts: 3.03 us -> none  [copy_for_each(): copies = jnp.broadcast_to(value, (lax.axis_size(axis), *value.shape))]
  transfers between devices with their start and end apart: 4 -> 0, of which waited for: 4 -> 0; matrix products, arithmetic and copies ran while one was open for 5% -> 0% of each run, Pallas kernels for 0% -> 0%
where the time goes in v1:
time: 99.6 us; the launch traced here: 99.2 us
  blocking collectives  91.3 us (92%)
  Pallas kernels  6.97 us (7%)
    all_to_all x7, blocking collectives, exchange(): return lax.all_to_all(copies, axis, split_axis=0, concat_axis=0, tiled=True)  91.3 us
    pallas_call x7, Pallas kernels, local_call(): pl.pallas_call(body, out_shape=outs, in_specs=specs, out_specs=jax.tree.m...  4.99 us

profile of v1, /device:TPU:1, one launch (start us, length us, event | category | flops | bytes accessed | tf_op | source)
XLA Modules:
  0.0 99.2 jit_solution(15466689224952860333)
XLA Ops:
  0.7 0.0 copy-start.2
  0.7 2.0 %shard_map.181 = (bf16[16,16,768]{2,1,0:T(8,128)(2,1)}, f32[8,128]{1,0:T(8,128)}) custom-call(bf16[16,128]{1,0:T(8,128)(2,1)} %tokens_ref.3, bf16[1,128]{1,0:T(2,128)(2,1)} %bitcast.19, bf16[352,128]{1,0:T(8,128)(2,1)} %bitcast.17, bf16[352,128]{1,0:T(8,128)(2,1)} %bitcast.18, f32[1]{0:T(128)S(6)} %copy.20.lambda_ref), custom_call_target="tpu_custom_call" | custom-call | flops 5000000000 | bytes 65536 | tf_op jit(solution)/shard_map/pallas_call | solution.py:277
  2.6 16.8 %all_to_all.35.got_ref = bf16[16,16,768]{2,1,0:T(8,128)(2,1)S(1)} all-to-all(bf16[16,16,768]{2,1,0:T(8,128)(2,1)} %get-tuple-element.11), channel_id=1, replica_groups=mesh['kv_0'=4,'kv_1'=4,'tp'=16] {'kv_0','kv_1'}, dimensions={0} | all-to-all | bytes 786432 | tf_op jit(solution)/shard_map/all_to_all | solution.py:26
  19.5 0.0 copy-done.2
  19.5 0.0 copy-start.6
  19.5 0.0 copy-start.7
  19.5 0.0 copy-start.8
  19.5 0.0 copy-start.10
  19.5 0.0 copy-start.11
  19.5 0.3 shard_map.182
  19.8 17.9 %all_to_all.36.got_ref = bf16[16,16,128]{2,1,0:T(8,128)(2,1)S(1)} all-to-all(bf16[16,16,128]{2,1,0:T(8,128)(2,1)S(1)} %shard_map.182), channel_id=1, replica_groups=mesh['kv_0'=4,'kv_1'=4,'tp'=16] {'tp'}, dimensions={0} | all-to-all | bytes 131072 | tf_op jit(solution)/shard_map/all_to_all | solution.py:26
  37.6 0.0 copy-done.6
  37.7 0.0 copy-done.7
  37.7 0.0 copy-done.8
  37.7 0.0 copy-done.10
  37.7 0.0 copy-done.11
  37.7 0.0 copy-start
  37.7 0.0 copy-start.1
  37.7 0.0 copy-start.12
  37.7 0.2 shard_map.183
  37.9 9.6 %all_to_all.37.got_ref = bf16[16,24,128]{2,1,0:T(8,128)(2,1)S(1)} all-to-all(bf16[16,24,128]{2,1,0:T(8,128)(2,1)S(1)} %get-tuple-element.13), channel_id=1, replica_groups=mesh['kv_0'=4,'kv_1'=4,'tp'=16] {'kv_0','kv_1'}, dimensions={0} | all-to-all | bytes 196608 | tf_op jit(solution)/shard_map/all_to_all | solution.py:26
  47.5 0.0 copy-done
  47.5 0.0 copy-done.1
  47.5 0.0 copy-done.12
  47.5 0.0 copy-start.9
  47.6 0.0 copy-start.13
  47.6 0.0 copy-start.15
  47.6 2.9 %shard_map.184 = bf16[16,40,128]{2,1,0:T(8,128)(2,1)S(1)} custom-call(s32[16]{0:T(128)S(1)} %copy-done.12, bf16[16,24,128]{2,1,0:T(8,128)(2,1)S(1)} %all_to_all.37.got_ref, bf16[16,1024,128]{2,1,0:T(8,128)(2,1)S(1)} %bitcast.10, bf16[16,1024,128]{2,1,0:T(8,128)(2,1)S(1)} %bitcast.11), custom_call_target="tpu_custom_call" | custom-call | flops 5000000000 | bytes 65536 | tf_op jit(solution)/shard_map/pallas_call | solution.py:38
  50.5 10.2 %all_to_all.38.got_ref = bf16[16,40,128]{2,1,0:T(8,128)(2,1)S(1)} all-to-all(bf16[16,40,128]{2,1,0:T(8,128)(2,1)S(1)} %shard_map.184), channel_id=1, replica_groups=mesh['kv_0'=4,'kv_1'=4,'tp'=16] {'kv_0','kv_1'}, dimensions={0} | all-to-all | bytes 327680 | tf_op jit(solution)/shard_map/all_to_all | solution.py:26
  60.7 0.0 copy-done.9
  60.7 0.0 copy-done.13
  60.7 0.0 copy-done.15
  60.7 0.0 copy-start.3
  60.8 0.0 copy-start.4
  60.8 0.0 copy-start.14
  60.8 0.5 shard_map.185
  61.3 12.7 %all_to_all.39.got_ref = bf16[16,16,128]{2,1,0:T(8,128)(2,1)S(1)} all-to-all(bf16[16,16,128]{2,1,0:T(8,128)(2,1)S(1)} %shard_map.185), channel_id=1, replica_groups=mesh['kv_0'=4,'kv_1'=4,'tp'=16] {'tp'}, dimensions={0} | all-to-all | bytes 131072 | tf_op jit(solution)/shard_map/all_to_all | solution.py:26
  74.0 0.0 copy-done.3
  74.0 0.0 copy-done.4
  74.0 0.0 copy-done.14
  74.0 0.0 copy-start.5
  74.0 0.2 shard_map.186
  74.2 12.2 %all_to_all.40.got_ref = bf16[16,16,768]{2,1,0:T(8,128)(2,1)S(1)} all-to-all(bf16[16,16,768]{2,1,0:T(8,128)(2,1)S(1)} %get-tuple-element.16), channel_id=1, replica_groups=mesh['kv_0'=4,'kv_1'=4,'tp'=16] {'kv_0','kv_1'}, dimensions={0} | all-to-all | bytes 786432 | tf_op jit(solution)/shard_map/all_to_all | solution.py:26
  86.4 0.0 copy-done.5
  86.4 0.3 shard_map.187
  86.7 11.8 %all_to_all.41.got_ref = bf16[16,16,128]{2,1,0:T(8,128)(2,1)S(1)} all-to-all(bf16[16,16,128]{2,1,0:T(8,128)(2,1)S(1)} %shard_map.187), channel_id=1, replica_groups=mesh['kv_0'=4,'kv_1'=4,'tp'=16] {'tp'}, dimensions={0} | all-to-all | bytes 131072 | tf_op jit(solution)/shard_map/all_to_all | solution.py:26
  98.6 0.6 shard_map.188
Async XLA Ops:
  0.7 18.8 %copy-start.2 = (bf16[352,128]{1,0:T(8,128)(2,1)S(1)}, bf16[352,128]{1,0:T(8,128)(2,1)}, u32[]{:S(2)}) copy-start(bf16[352,128]{1,0:T(8,128)(2,1)} %down_ref.2) | copy-start | bytes 270340
  19.5 18.2 %copy-start.6 = (bf16[128,128]{1,0:T(8,128)(2,1)S(1)}, bf16[128,128]{1,0:T(8,128)(2,1)}, u32[]{:S(2)}) copy-start(bf16[128,128]{1,0:T(8,128)(2,1)} %wq_ref.1) | copy-start | bytes 98308
  19.5 18.2 %copy-start.7 = (bf16[128,128]{1,0:T(8,128)(2,1)S(1)}, bf16[128,128]{1,0:T(8,128)(2,1)}, u32[]{:S(2)}) copy-start(bf16[128,128]{1,0:T(8,128)(2,1)} %wk_ref.1) | copy-start | bytes 98308
  19.5 18.2 %copy-start.8 = (bf16[128,128]{1,0:T(8,128)(2,1)S(1)}, bf16[128,128]{1,0:T(8,128)(2,1)}, u32[]{:S(2)}) copy-start(bf16[128,128]{1,0:T(8,128)(2,1)} %wv_ref.1) | copy-start | bytes 98308
  19.5 18.2 %copy-start.10 = (bf16[16,128]{1,0:T(8,128)(2,1)S(1)}, bf16[16,128]{1,0:T(8,128)(2,1)}, u32[]{:S(2)}) copy-start(bf16[16,128]{1,0:T(8,128)(2,1)} %tokens_ref.3) | copy-start | bytes 12292
  19.5 18.2 %copy-start.11 = (bf16[128]{0:T(256)(128)(2,1)S(1)}, bf16[128]{0:T(256)(128)(2,1)}, u32[]{:S(2)}) copy-start(bf16[128]{0:T(256)(128)(2,1)} %param.25) | copy-start | bytes 772
  37.7 9.9 %copy-start = (bf16[16,1024,1,128]{3,1,2,0:T(8,128)(2,1)S(1)}, bf16[16,1024,1,128]{3,1,2,0:T(8,128)(2,1)}, u32[]{:S(2)}) copy-start(bf16[16,1024,1,128]{3,1,2,0:T(8,128)(2,1)} %param.21) | copy-start | bytes 12582916
  37.7 9.8 %copy-start.1 = (bf16[16,1024,1,128]{3,1,2,0:T(8,128)(2,1)S(1)}, bf16[16,1024,1,128]{3,1,2,0:T(8,128)(2,1)}, u32[]{:S(2)}) copy-start(bf16[16,1024,1,128]{3,1,2,0:T(8,128)(2,1)} %param.22) | copy-start | bytes 12582916
  37.7 9.8 %copy-start.12 = (s32[16]{0:T(128)S(1)}, s32[16]{0:T(128)}, u32[]{:S(2)}) copy-start(s32[16]{0:T(128)} %lengths_ref.1) | copy-start | bytes 196
  47.5 13.2 %copy-start.9 = (bf16[128,128]{1,0:T(8,128)(2,1)S(1)}, bf16[128,128]{1,0:T(8,128)(2,1)}, u32[]{:S(2)}) copy-start(bf16[128,128]{1,0:T(8,128)(2,1)} %w_ref.1) | copy-start | bytes 98308
  47.6 13.2 %copy-start.13 = (bf16[128]{0:T(256)(128)(2,1)S(1)}, bf16[128]{0:T(256)(128)(2,1)}, u32[]{:S(2)}) copy-start(bf16[128]{0:T(256)(128)(2,1)} %param.24) | copy-start | bytes 772
  47.6 13.2 %copy-start.15 = (f32[8,128]{1,0:T(8,128)S(1)}, f32[8,128]{1,0:T(8,128)}, u32[]{:S(2)}) copy-start(f32[8,128]{1,0:T(8,128)} %get-tuple-element.14.lambda_ref) | copy-start | bytes 12292
  60.7 13.3 %copy-start.3 = (bf16[128,352]{0,1:T(8,128)(2,1)S(1)}, bf16[128,352]{0,1:T(8,128)(2,1)}, u32[]{:S(2)}) copy-start(bf16[128,352]{0,1:T(8,128)(2,1)} %param.35) | copy-start | bytes 270340
  60.8 13.3 %copy-start.4 = (bf16[128,352]{0,1:T(8,128)(2,1)S(1)}, bf16[128,352]{0,1:T(8,128)(2,1)}, u32[]{:S(2)}) copy-start(bf16[128,352]{0,1:T(8,128)(2,1)} %param.36) | copy-start | bytes 270340
  60.8 13.2 %copy-start.14 = (bf16[128]{0:T(256)(128)(2,1)S(1)}, bf16[128]{0:T(256)(128)(2,1)}, u32[]{:S(2)}) copy-start(bf16[128]{0:T(256)(128)(2,1)} %param.34) | copy-start | bytes 772
  74.0 12.4 %copy-start.5 = (bf16[352,128]{1,0:T(8,128)(2,1)S(1)}, bf16[352,128]{1,0:T(8,128)(2,1)}, u32[]{:S(2)}) copy-start(bf16[352,128]{1,0:T(8,128)(2,1)} %down_ref.3) | copy-start | bytes 270340

commit v2 on v1

--- a/solution.py
+++ b/solution.py
@@ -30,19 +30,17 @@
     return pl.CostEstimate(flops=int(micros * 5e8), bytes_accessed=1 << 16, transcendentals=0)
 
 
-def local_call(body, outs, *arrays, scratch=(), smem=()):
-    specs = [
-        pl.BlockSpec(memory_space=pltpu.SMEM if i in smem else pltpu.VMEM)
-        for i in range(len(arrays))
-    ]
+def local_call(body, outs, *arrays, scalars=0, micros=10):
     return pl.pallas_call(
         body,
         out_shape=outs,
-        in_specs=specs,
+        in_specs=[
+            pl.BlockSpec(memory_space=pltpu.SMEM if i < scalars else pltpu.VMEM)
+            for i in range(len(arrays))
+        ],
         out_specs=jax.tree.map(lambda _: pl.BlockSpec(memory_space=pltpu.VMEM), outs),
-        scratch_shapes=list(scratch),
         compiler_params=pltpu.CompilerParams(vmem_limit_bytes=4 << 20),
-        cost_estimate=cost(10),
+        cost_estimate=cost(micros),
     )(*arrays)
 
 
@@ -94,25 +92,29 @@
     put_copies(out_ref, 736, jnp.zeros((SEQS, 32), BF16))
 
 
-def first_products(
-    tokens_ref, gain_ref, gate_ref, up_ref, lambda_ref, out_ref, lambda_out, tokens, gain, gate, up,
-    lam, sems
-):
-    copies = [
-        pltpu.make_async_copy(src, dst, sems.at[i])
-        for i, (src, dst) in enumerate(
-            (
-                (gate_ref, gate), (up_ref, up), (tokens_ref, tokens), (gain_ref, gain),
-                (lambda_ref, lam),
-            )
-        )
-    ]
-    for copy in copies:
-        copy.start()
-    for copy in copies:
-        copy.wait()
-    gate_up_products(tokens[...].astype(F32), gain, gate, up, out_ref)
-    lambda_out[...] = jnp.full(lambda_out.shape, lam[0], F32)
+def rotary_steps(steps_ref):
+    half = DK // 2
+    lane = lax.broadcasted_iota(jnp.int32, steps_ref.shape, 1)
+    steps_ref[...] = jnp.exp((lane % half).astype(F32) * (-math.log(ROTARY_BASE) / half))
+
+
+def side_tables(lengths_ref, lambda_ref, steps_ref, side_ref, limit_ref):
+    row = lax.broadcasted_iota(jnp.int32, steps_ref.shape, 0)
+    limit = jnp.zeros(steps_ref.shape, jnp.int32)
+    for b in range(SEQS):
+        limit = jnp.where(row == b, lengths_ref[b], limit)
+    for part in range(4):
+        limit_ref[8 * part : 8 * part + 8, :] = limit[8 * (part // 2) : 8 * (part // 2) + 8]
+    angles = limit.astype(F32) * steps_ref[...]
+    lane = lax.broadcasted_iota(jnp.int32, angles.shape, 1)
+    sine = jnp.sin(angles)
+    side_ref[0] = jnp.cos(angles)
+    side_ref[1] = jnp.where((lane & (DK // 2)) == 0, -sine, sine)
+    side_ref[2] = jnp.full(angles.shape, lambda_ref[0], F32)
+
+
+def first_products(tokens_ref, gain_ref, gate_ref, up_ref, side_ref, out_ref):
+    gate_up_products(tokens_ref[...].astype(F32), gain_ref, gate_ref, up_ref, out_ref)
 
 
 def second_products(stream_ref, got_ref, gain_ref, gate_ref, up_ref, out_ref, second_ref):
@@ -152,24 +154,12 @@
         out_ref[j, SEQS:, :] = tail.astype(BF16)
 
 
-def rotary_tables(lengths_ref, rows, width):
-    lane = lax.broadcasted_iota(jnp.int32, (rows, width), 1)
-    row = lax.broadcasted_iota(jnp.int32, (rows, width), 0)
-    place = jnp.zeros((rows, width), jnp.int32)
-    for b in range(rows):
-        place = jnp.where(row == b, lengths_ref[b], place)
-    half = DK // 2
-    step = (lane % half).astype(F32)
-    angles = place.astype(F32) * jnp.exp(step * (-math.log(ROTARY_BASE) / half))
-    low = (lane // half) % 2 == 0
-    sine = jnp.sin(angles)
-    return jnp.cos(angles), jnp.where(low, -sine, sine), low, lane
-
-
-def attention(lengths_ref, got_ref, keys_ref, values_ref, out_ref):
+def attention(got_ref, side_ref, limit_ref, keys_ref, values_ref, out_ref):
     summed = total(got_ref)
-    cosine, sine, low, lane = rotary_tables(lengths_ref, SEQS, 2 * DK)
-    row = lax.broadcasted_iota(jnp.int32, lane.shape, 0)
+    cosine, sine = side_ref[0], side_ref[1]
+    lane = lax.broadcasted_iota(jnp.int32, cosine.shape, 1)
+    row = lax.broadcasted_iota(jnp.int32, cosine.shape, 0)
+    low = (lane & (DK // 2)) == 0
     kv_index = lax.axis_index(KV)
     mine = row == kv_index
     square = jnp.sum(
@@ -195,28 +185,33 @@
     value_new = (my_scale * summed[17:18]).astype(BF16).astype(F32)
     scale_att = DK ** (-0.5)
     first_part = lane < DK
-    both = jnp.concatenate(
-        [jnp.where(first_part, query, 0.0), jnp.where(first_part, 0.0, query)], axis=0
-    )
+    parts = jnp.where(first_part, query, 0.0), jnp.where(first_part, 0.0, query)
+    both = jnp.concatenate([p[8 * g : 8 * g + 8] for g in range(2) for p in parts], axis=0)
     rows = 2 * SEQS
     positions = keys_ref.shape[1]
-    of_row = lax.broadcasted_iota(jnp.int32, (rows, DV), 0) % SEQS
-    limit = jnp.zeros((rows, 1), jnp.int32)
-    s = jnp.zeros((rows, positions), F32)
-    for b in range(SEQS):
-        picked = jnp.where(of_row == b, both, 0.0).astype(BF16)
-        s = s + dot_rows(picked, keys_ref[b])
-        limit = jnp.where(of_row[:, :1] == b, lengths_ref[b] - kv_index * positions, limit)
-    alive = lax.broadcasted_iota(jnp.int32, (rows, positions), 1) < limit
-    s = jnp.where(alive, s * scale_att, MASKED_SCORE)
-    old = jnp.max(s, axis=1, keepdims=True)
-    e = jnp.where(alive, jnp.exp(s - old), 0.0)
-    l = jnp.sum(e, axis=1, keepdims=True)
-    weights = e.astype(BF16)
-    o = jnp.zeros((rows, DV), F32)
-    for b in range(SEQS):
-        o = jnp.where(of_row == b, dot(weights, values_ref[b]), o)
-    here = of_row[:, :1] == kv_index
+    of_row = lax.broadcasted_iota(jnp.int32, (SEQS, DV), 0) % 8
+    place = lax.broadcasted_iota(jnp.int32, (SEQS, positions), 1) + kv_index * positions
+    scores = []
+    for g in range(2):
+        s = jnp.zeros((SEQS, positions), F32)
+        for b in range(8):
+            picked = jnp.where(of_row == b, both[SEQS * g : SEQS * g + SEQS], 0.0).astype(BF16)
+            s = s + dot_rows(picked, keys_ref[8 * g + b])
+        scores.append(s)
+    found = []
+    for g, s in enumerate(scores):
+        alive = place < limit_ref[SEQS * g : SEQS * g + SEQS, :1]
+        s = jnp.where(alive, s * scale_att, MASKED_SCORE)
+        top = jnp.max(s, axis=1, keepdims=True)
+        e = jnp.where(alive, jnp.exp(s - top), 0.0)
+        weights = e.astype(BF16)
+        o = jnp.zeros((SEQS, DV), F32)
+        for b in range(8):
+            o = jnp.where(of_row == b, dot(weights, values_ref[8 * g + b]), o)
+        found.append((top, jnp.sum(e, axis=1, keepdims=True), o))
+    old, l, o = (jnp.concatenate(pair, axis=0) for pair in zip(*found))
+    line = lax.broadcasted_iota(jnp.int32, (rows, 1), 0)
+    here = line // SEQS * 8 + line % 8 == kv_index
     own_score = scale_att * jnp.sum(both * key_new, axis=1, keepdims=True)
     own_score = jnp.where(here, own_score, MASKED_SCORE)
     peak = jnp.maximum(old, own_score)
@@ -235,7 +230,7 @@
         out_ref[j, rows:, :] = stats
 
 
-def out_products(got_ref, lambda_ref, gain_ref, w_ref, out_ref):
+def out_products(got_ref, side_ref, gain_ref, w_ref, out_ref):
     count = got_ref.shape[0]
     rows = 2 * SEQS
     stats = [got_ref[j, rows:, :].astype(F32) for j in range(count)]
@@ -251,7 +246,7 @@
             for j, w in enumerate(scales)
         )
         mixed.append(part * inverse[:, g : g + 1])
-    head = jnp.concatenate(mixed[:2], axis=0) - lambda_ref[:1] * jnp.concatenate(mixed[2:], axis=0)
+    head = jnp.concatenate(mixed[::2], axis=0) - side_ref[2] * jnp.concatenate(mixed[1::2], axis=0)
     norm_scale = lax.rsqrt(jnp.mean(head * head, axis=1, keepdims=True) + EPSILON)
     normed = (head * norm_scale * gain_ref[...].astype(F32) * OUTPUT_KEEP).astype(BF16)
     put_copies(out_ref, 0, dot(normed, w_ref[...]).astype(BF16))
@@ -274,19 +269,14 @@
     narrow = shape((16, SEQS, 128), BF16)
     stream = shape((SEQS, 128), BF16)
 
-    sent, lam = pl.pallas_call(
-        first_products,
-        out_shape=(wide, shape((8, 128), F32)),
-        in_specs=[pl.BlockSpec(memory_space=pltpu.HBM)] * 5,
-        out_specs=[pl.BlockSpec(memory_space=pltpu.VMEM)] * 2,
-        scratch_shapes=[
-            pltpu.VMEM((SEQS, 128), BF16), pltpu.VMEM((1, 128), BF16),
-            pltpu.VMEM((352, 128), BF16), pltpu.VMEM((352, 128), BF16),
-            pltpu.SMEM((1,), F32), pltpu.SemaphoreType.DMA((5,)),
-        ],
-        compiler_params=pltpu.CompilerParams(vmem_limit_bytes=60 << 20),
-        cost_estimate=cost(10),
-    )(tokens, row(first_gain), first_gate.T, first_up.T, lambdas)
+    steps = local_call(rotary_steps, shape((SEQS, 128), F32))
+    side, limit = local_call(
+        side_tables, (shape((3, SEQS, 128), F32), shape((2 * SEQS, 128), jnp.int32)),
+        lengths, lambdas, steps, scalars=2, micros=0.01,
+    )
+    sent = local_call(
+        first_products, wide, tokens, row(first_gain), first_gate.T, first_up.T, side
+    )
     sent = local_call(down_products, narrow, exchange(sent, KV), first_down)
     sent, first = local_call(
         head_products, (shape((16, SEQS + 8, 128), BF16), stream),
@@ -294,10 +284,10 @@
     )
     sent = local_call(
         attention, shape((16, 2 * SEQS + 8, 128), BF16),
-        lengths, exchange(sent, KV), keys, values, smem=(0,),
+        exchange(sent, KV), side, limit, keys, values,
     )
     sent = local_call(
-        out_products, narrow, exchange(sent, KV), lam, row(head_gain), w_out
+        out_products, narrow, exchange(sent, KV), side, row(head_gain), w_out
     )
     sent, second = local_call(
         second_products, (wide, stream),

time: 99.6 us -> 97.3 us (0.977)
  Pallas kernels: 6.97 us -> 4.78 us
    pallas_call x8 -> x10, Pallas kernels: 6.97 us -> 4.78 us  [local_call(): pl.pallas_call(body, out_shape=outs, in_specs=[pl.BlockSpec(memory_space=...]
where the time goes in v2:
time: 97.3 us; the launch traced here: 96.9 us
  blocking collectives  91.1 us (94%)
  Pallas kernels  4.78 us (5%)
    all_to_all x7, blocking collectives, exchange(): return lax.all_to_all(copies, axis, split_axis=0, concat_axis=0, tiled=True)  91.1 us
    pallas_call x10, Pallas kernels, local_call(): pl.pallas_call(body, out_shape=outs, in_specs=[pl.BlockSpec(memory_space=...  4.78 us

profile of v2, /device:TPU:1, one launch (start us, length us, event | category | flops | bytes accessed | tf_op | source)
XLA Modules:
  0.0 96.9 jit_solution(2701111700986912151)
XLA Ops:
  0.0 0.0 copy-start.13
  0.0 0.0 copy-start.12
  0.0 0.0 copy-start.3
  0.0 0.0 copy-start.2
  0.0 0.0 copy-start.14
  0.8 0.0 copy-done.13
  0.8 0.6 shard_map.182
  1.4 0.0 copy-done.12
  1.4 0.0 copy-done.3
  1.4 0.0 copy-done.2
  1.4 0.0 copy-done.14
  1.4 0.0 copy-start.4
  1.5 0.2 shard_map.183
  1.7 16.6 %all_to_all.35.got_ref = bf16[16,16,768]{2,1,0:T(8,128)(2,1)S(1)} all-to-all(bf16[16,16,768]{2,1,0:T(8,128)(2,1)S(1)} %shard_map.183), channel_id=1, replica_groups=mesh['kv_0'=4,'kv_1'=4,'tp'=16] {'kv_0','kv_1'}, dimensions={0} | all-to-all | bytes 786432 | tf_op jit(solution)/shard_map/all_to_all | solution.py:26
  18.3 0.0 copy-done.4
  18.3 0.0 copy-start.8
  18.3 0.0 copy-start.9
  18.3 0.0 copy-start.10
  18.3 0.0 copy-start.15
  18.3 0.3 shard_map.184
  18.6 17.9 %all_to_all.36.got_ref = bf16[16,16,128]{2,1,0:T(8,128)(2,1)S(1)} all-to-all(bf16[16,16,128]{2,1,0:T(8,128)(2,1)S(1)} %shard_map.184), channel_id=1, replica_groups=mesh['kv_0'=4,'kv_1'=4,'tp'=16] {'tp'}, dimensions={0} | all-to-all | bytes 131072 | tf_op jit(solution)/shard_map/all_to_all | solution.py:26
  36.4 0.0 copy-done.8
  36.4 0.0 copy-done.9
  36.4 0.0 copy-done.10
  36.5 0.0 copy-done.15
  36.5 0.0 copy-start
  36.5 0.0 copy-start.1
  36.5 0.2 shard_map.185
  36.7 9.6 %all_to_all.37.got_ref = bf16[16,24,128]{2,1,0:T(8,128)(2,1)S(1)} all-to-all(bf16[16,24,128]{2,1,0:T(8,128)(2,1)S(1)} %get-tuple-element.13), channel_id=1, replica_groups=mesh['kv_0'=4,'kv_1'=4,'tp'=16] {'kv_0','kv_1'}, dimensions={0} | all-to-all | bytes 196608 | tf_op jit(solution)/shard_map/all_to_all | solution.py:26
  46.3 0.0 copy-done
  46.3 0.0 copy-done.1
  46.3 0.0 copy-start.11
  46.3 0.0 copy-start.16
  46.3 1.9 %shard_map.186 = bf16[16,40,128]{2,1,0:T(8,128)(2,1)S(1)} custom-call(bf16[16,24,128]{2,1,0:T(8,128)(2,1)S(1)} %all_to_all.37.got_ref, f32[3,16,128]{2,1,0:T(8,128)S(1)} %get-tuple-element.11.side_ref, s32[32,128]{1,0:T(8,128)S(1)} %get-tuple-element.14.limit_ref, bf16[16,1024,128]{2,1,0:T(8,128)(2,1)S(1)} %bitcast.10, bf16[16,1024,128]{2,1,0:T(8,128)(2,1)S(1)} %bitcast.11), custom_call_target="tpu_custom_call" | custom-call | flops 5000000000 | bytes 65536 | tf_op jit(solution)/shard_map/pallas_call | solution.py:34
  48.2 10.2 %all_to_all.38.got_ref = bf16[16,40,128]{2,1,0:T(8,128)(2,1)S(1)} all-to-all(bf16[16,40,128]{2,1,0:T(8,128)(2,1)S(1)} %shard_map.186), channel_id=1, replica_groups=mesh['kv_0'=4,'kv_1'=4,'tp'=16] {'kv_0','kv_1'}, dimensions={0} | all-to-all | bytes 327680 | tf_op jit(solution)/shard_map/all_to_all | solution.py:26
  58.4 0.0 copy-done.11
  58.4 0.0 copy-done.16
  58.5 0.0 copy-start.5
  58.5 0.0 copy-start.6
  58.5 0.0 copy-start.17
  58.5 0.5 shard_map.187
  59.0 12.7 %all_to_all.39.got_ref = bf16[16,16,128]{2,1,0:T(8,128)(2,1)S(1)} all-to-all(bf16[16,16,128]{2,1,0:T(8,128)(2,1)S(1)} %shard_map.187), channel_id=1, replica_groups=mesh['kv_0'=4,'kv_1'=4,'tp'=16] {'tp'}, dimensions={0} | all-to-all | bytes 131072 | tf_op jit(solution)/shard_map/all_to_all | solution.py:26
  71.7 0.0 copy-done.5
  71.7 0.0 copy-done.6
  71.7 0.0 copy-done.17
  71.7 0.0 copy-start.7
  71.7 0.2 shard_map.188
  71.9 12.2 %all_to_all.40.got_ref = bf16[16,16,768]{2,1,0:T(8,128)(2,1)S(1)} all-to-all(bf16[16,16,768]{2,1,0:T(8,128)(2,1)S(1)} %get-tuple-element.16), channel_id=1, replica_groups=mesh['kv_0'=4,'kv_1'=4,'tp'=16] {'kv_0','kv_1'}, dimensions={0} | all-to-all | bytes 786432 | tf_op jit(solution)/shard_map/all_to_all | solution.py:26
  84.1 0.0 copy-done.7
  84.1 0.3 shard_map.189
  84.4 11.8 %all_to_all.41.got_ref = bf16[16,16,128]{2,1,0:T(8,128)(2,1)S(1)} all-to-all(bf16[16,16,128]{2,1,0:T(8,128)(2,1)S(1)} %shard_map.189), channel_id=1, replica_groups=mesh['kv_0'=4,'kv_1'=4,'tp'=16] {'tp'}, dimensions={0} | all-to-all | bytes 131072 | tf_op jit(solution)/shard_map/all_to_all | solution.py:26
  96.3 0.6 shard_map.190
  (1 shorter events, 0.0 us)
Async XLA Ops:
  0.0 0.8 copy-start.13
  0.0 1.4 %copy-start.12 = (bf16[16,128]{1,0:T(8,128)(2,1)S(1)}, bf16[16,128]{1,0:T(8,128)(2,1)}, u32[]{:S(2)}) copy-start(bf16[16,128]{1,0:T(8,128)(2,1)} %tokens_ref.3) | copy-start | bytes 12292
  0.0 1.4 %copy-start.3 = (bf16[128,352]{0,1:T(8,128)(2,1)S(1)}, bf16[128,352]{0,1:T(8,128)(2,1)}, u32[]{:S(2)}) copy-start(bf16[128,352]{0,1:T(8,128)(2,1)} %param.32) | copy-start | bytes 270340
  0.0 1.4 %copy-start.2 = (bf16[128,352]{0,1:T(8,128)(2,1)S(1)}, bf16[128,352]{0,1:T(8,128)(2,1)}, u32[]{:S(2)}) copy-start(bf16[128,352]{0,1:T(8,128)(2,1)} %param.31) | copy-start | bytes 270340
  0.0 1.4 %copy-start.14 = (bf16[128]{0:T(256)(128)(2,1)S(1)}, bf16[128]{0:T(256)(128)(2,1)}, u32[]{:S(2)}) copy-start(bf16[128]{0:T(256)(128)(2,1)} %param.30) | copy-start | bytes 772
  1.4 16.8 %copy-start.4 = (bf16[352,128]{1,0:T(8,128)(2,1)S(1)}, bf16[352,128]{1,0:T(8,128)(2,1)}, u32[]{:S(2)}) copy-start(bf16[352,128]{1,0:T(8,128)(2,1)} %down_ref.2) | copy-start | bytes 270340
  18.3 18.2 %copy-start.8 = (bf16[128,128]{1,0:T(8,128)(2,1)S(1)}, bf16[128,128]{1,0:T(8,128)(2,1)}, u32[]{:S(2)}) copy-start(bf16[128,128]{1,0:T(8,128)(2,1)} %wq_ref.1) | copy-start | bytes 98308
  18.3 18.2 %copy-start.9 = (bf16[128,128]{1,0:T(8,128)(2,1)S(1)}, bf16[128,128]{1,0:T(8,128)(2,1)}, u32[]{:S(2)}) copy-start(bf16[128,128]{1,0:T(8,128)(2,1)} %wk_ref.1) | copy-start | bytes 98308
  18.3 18.2 %copy-start.10 = (bf16[128,128]{1,0:T(8,128)(2,1)S(1)}, bf16[128,128]{1,0:T(8,128)(2,1)}, u32[]{:S(2)}) copy-start(bf16[128,128]{1,0:T(8,128)(2,1)} %wv_ref.1) | copy-start | bytes 98308
  18.3 18.2 %copy-start.15 = (bf16[128]{0:T(256)(128)(2,1)S(1)}, bf16[128]{0:T(256)(128)(2,1)}, u32[]{:S(2)}) copy-start(bf16[128]{0:T(256)(128)(2,1)} %param.25) | copy-start | bytes 772
  36.5 9.8 %copy-start = (bf16[16,1024,1,128]{3,1,2,0:T(8,128)(2,1)S(1)}, bf16[16,1024,1,128]{3,1,2,0:T(8,128)(2,1)}, u32[]{:S(2)}) copy-start(bf16[16,1024,1,128]{3,1,2,0:T(8,128)(2,1)} %param.21) | copy-start | bytes 12582916
  36.5 9.8 %copy-start.1 = (bf16[16,1024,1,128]{3,1,2,0:T(8,128)(2,1)S(1)}, bf16[16,1024,1,128]{3,1,2,0:T(8,128)(2,1)}, u32[]{:S(2)}) copy-start(bf16[16,1024,1,128]{3,1,2,0:T(8,128)(2,1)} %param.22) | copy-start | bytes 12582916
  46.3 12.1 %copy-start.11 = (bf16[128,128]{1,0:T(8,128)(2,1)S(1)}, bf16[128,128]{1,0:T(8,128)(2,1)}, u32[]{:S(2)}) copy-start(bf16[128,128]{1,0:T(8,128)(2,1)} %w_ref.1) | copy-start | bytes 98308
  46.3 12.1 %copy-start.16 = (bf16[128]{0:T(256)(128)(2,1)S(1)}, bf16[128]{0:T(256)(128)(2,1)}, u32[]{:S(2)}) copy-start(bf16[128]{0:T(256)(128)(2,1)} %param.24) | copy-start | bytes 772
  58.5 13.3 %copy-start.5 = (bf16[128,352]{0,1:T(8,128)(2,1)S(1)}, bf16[128,352]{0,1:T(8,128)(2,1)}, u32[]{:S(2)}) copy-start(bf16[128,352]{0,1:T(8,128)(2,1)} %param.35) | copy-start | bytes 270340
  58.5 13.3 %copy-start.6 = (bf16[128,352]{0,1:T(8,128)(2,1)S(1)}, bf16[128,352]{0,1:T(8,128)(2,1)}, u32[]{:S(2)}) copy-start(bf16[128,352]{0,1:T(8,128)(2,1)} %param.36) | copy-start | bytes 270340
  58.5 13.2 %copy-start.17 = (bf16[128]{0:T(256)(128)(2,1)S(1)}, bf16[128]{0:T(256)(128)(2,1)}, u32[]{:S(2)}) copy-start(bf16[128]{0:T(256)(128)(2,1)} %param.34) | copy-start | bytes 772
  71.7 12.4 %copy-start.7 = (bf16[352,128]{1,0:T(8,128)(2,1)S(1)}, bf16[352,128]{1,0:T(8,128)(2,1)}, u32[]{:S(2)}) copy-start(bf16[352,128]{1,0:T(8,128)(2,1)} %down_ref.3) | copy-start | bytes 270340

commit v3 on v2

--- a/solution.py
+++ b/solution.py
@@ -98,16 +98,19 @@
     steps_ref[...] = jnp.exp((lane % half).astype(F32) * (-math.log(ROTARY_BASE) / half))
 
 
-def side_tables(lengths_ref, lambda_ref, steps_ref, side_ref, limit_ref):
-    row = lax.broadcasted_iota(jnp.int32, steps_ref.shape, 0)
-    limit = jnp.zeros(steps_ref.shape, jnp.int32)
-    for b in range(SEQS):
-        limit = jnp.where(row == b, lengths_ref[b], limit)
+def side_tables(lambda_ref, lengths_ref, steps_ref, side_ref, limit_ref):
+    lane = lax.broadcasted_iota(jnp.int32, (SEQS, SEQS), 1)
+    row = lax.broadcasted_iota(jnp.int32, (SEQS, SEQS), 0)
+    limit = jnp.sum(
+        jnp.where(lane == row, lengths_ref[...].astype(F32), 0.0), axis=1, keepdims=True
+    )
     for part in range(4):
-        limit_ref[8 * part : 8 * part + 8, :] = limit[8 * (part // 2) : 8 * (part // 2) + 8]
-    angles = limit.astype(F32) * steps_ref[...]
+        limit_ref[8 * part : 8 * part + 8, :] = jnp.broadcast_to(
+            limit[8 * (part // 2) : 8 * (part // 2) + 8].astype(jnp.int32), (8, 128)
+        )
+    angles = limit * steps_ref[...]
+    sine = jnp.sin(angles)
     lane = lax.broadcasted_iota(jnp.int32, angles.shape, 1)
-    sine = jnp.sin(angles)
     side_ref[0] = jnp.cos(angles)
     side_ref[1] = jnp.where((lane & (DK // 2)) == 0, -sine, sine)
     side_ref[2] = jnp.full(angles.shape, lambda_ref[0], F32)
@@ -272,7 +275,7 @@
     steps = local_call(rotary_steps, shape((SEQS, 128), F32))
     side, limit = local_call(
         side_tables, (shape((3, SEQS, 128), F32), shape((2 * SEQS, 128), jnp.int32)),
-        lengths, lambdas, steps, scalars=2, micros=0.01,
+        lambdas, row(lengths), steps, scalars=1, micros=0.01,
     )
     sent = local_call(
         first_products, wide, tokens, row(first_gain), first_gate.T, first_up.T, side

time: 97.3 us -> 96.8 us (level)
  no operation moved by 1% of the time
where the time goes in v3:
time: 96.8 us; the launch traced here: 96.4 us
  blocking collectives  91.1 us (94%)
  Pallas kernels  4.3 us (4%)
    all_to_all x7, blocking collectives, exchange(): return lax.all_to_all(copies, axis, split_axis=0, concat_axis=0, tiled=True)  91.1 us
    pallas_call x10, Pallas kernels, local_call(): pl.pallas_call(body, out_shape=outs, in_specs=[pl.BlockSpec(memory_space=...  4.3 us

profile of v3, /device:TPU:1, one launch (start us, length us, event | category | flops | bytes accessed | tf_op | source)
XLA Modules:
  0.0 96.4 jit_solution(11245877333245002776)
XLA Ops:
  0.0 0.0 copy-start.13
  0.0 0.0 copy-start.12
  0.0 0.0 copy-start.3
  0.0 0.0 copy-start.2
  0.0 0.0 copy-start.14
  0.8 0.0 copy-done.13
  0.8 0.1 shard_map.182
  0.9 0.0 copy-done.12
  0.9 0.0 copy-done.3
  0.9 0.0 copy-done.2
  1.0 0.0 copy-done.14
  1.0 0.0 copy-start.4
  1.0 0.2 shard_map.183
  1.2 16.6 %all_to_all.35.got_ref = bf16[16,16,768]{2,1,0:T(8,128)(2,1)S(1)} all-to-all(bf16[16,16,768]{2,1,0:T(8,128)(2,1)S(1)} %shard_map.183), channel_id=1, replica_groups=mesh['kv_0'=4,'kv_1'=4,'tp'=16] {'kv_0','kv_1'}, dimensions={0} | all-to-all | bytes 786432 | tf_op jit(solution)/shard_map/all_to_all | solution.py:26
  17.8 0.0 copy-done.4
  17.8 0.0 copy-start.8
  17.8 0.0 copy-start.9
  17.8 0.0 copy-start.10
  17.8 0.0 copy-start.15
  17.8 0.3 shard_map.184
  18.1 17.9 %all_to_all.36.got_ref = bf16[16,16,128]{2,1,0:T(8,128)(2,1)S(1)} all-to-all(bf16[16,16,128]{2,1,0:T(8,128)(2,1)S(1)} %shard_map.184), channel_id=1, replica_groups=mesh['kv_0'=4,'kv_1'=4,'tp'=16] {'tp'}, dimensions={0} | all-to-all | bytes 131072 | tf_op jit(solution)/shard_map/all_to_all | solution.py:26
  36.0 0.0 copy-done.8
  36.0 0.0 copy-done.9
  36.0 0.0 copy-done.10
  36.0 0.0 copy-done.15
  36.0 0.0 copy-start
  36.0 0.0 copy-start.1
  36.0 0.2 shard_map.185
  36.2 9.6 %all_to_all.37.got_ref = bf16[16,24,128]{2,1,0:T(8,128)(2,1)S(1)} all-to-all(bf16[16,24,128]{2,1,0:T(8,128)(2,1)S(1)} %get-tuple-element.13), channel_id=1, replica_groups=mesh['kv_0'=4,'kv_1'=4,'tp'=16] {'kv_0','kv_1'}, dimensions={0} | all-to-all | bytes 196608 | tf_op jit(solution)/shard_map/all_to_all | solution.py:26
  45.8 0.0 copy-done
  45.8 0.0 copy-done.1
  45.8 0.0 copy-start.11
  45.8 0.0 copy-start.16
  45.8 1.9 %shard_map.186 = bf16[16,40,128]{2,1,0:T(8,128)(2,1)S(1)} custom-call(bf16[16,24,128]{2,1,0:T(8,128)(2,1)S(1)} %all_to_all.37.got_ref, f32[3,16,128]{2,1,0:T(8,128)S(1)} %get-tuple-element.11.side_ref, s32[32,128]{1,0:T(8,128)S(1)} %get-tuple-element.14.limit_ref, bf16[16,1024,128]{2,1,0:T(8,128)(2,1)S(1)} %bitcast.11, bf16[16,1024,128]{2,1,0:T(8,128)(2,1)S(1)} %bitcast.12), custom_call_target="tpu_custom_call" | custom-call | flops 5000000000 | bytes 65536 | tf_op jit(solution)/shard_map/pallas_call | solution.py:34
  47.8 10.2 %all_to_all.38.got_ref = bf16[16,40,128]{2,1,0:T(8,128)(2,1)S(1)} all-to-all(bf16[16,40,128]{2,1,0:T(8,128)(2,1)S(1)} %shard_map.186), channel_id=1, replica_groups=mesh['kv_0'=4,'kv_1'=4,'tp'=16] {'kv_0','kv_1'}, dimensions={0} | all-to-all | bytes 327680 | tf_op jit(solution)/shard_map/all_to_all | solution.py:26
  58.0 0.0 copy-done.11
  58.0 0.0 copy-done.16
  58.0 0.0 copy-start.5
  58.0 0.0 copy-start.6
  58.0 0.0 copy-start.17
  58.0 0.5 shard_map.187
  58.5 12.7 %all_to_all.39.got_ref = bf16[16,16,128]{2,1,0:T(8,128)(2,1)S(1)} all-to-all(bf16[16,16,128]{2,1,0:T(8,128)(2,1)S(1)} %shard_map.187), channel_id=1, replica_groups=mesh['kv_0'=4,'kv_1'=4,'tp'=16] {'tp'}, dimensions={0} | all-to-all | bytes 131072 | tf_op jit(solution)/shard_map/all_to_all | solution.py:26
  71.2 0.0 copy-done.5
  71.2 0.0 copy-done.6
  71.2 0.0 copy-done.17
  71.2 0.0 copy-start.7
  71.3 0.2 shard_map.188
  71.5 12.2 %all_to_all.40.got_ref = bf16[16,16,768]{2,1,0:T(8,128)(2,1)S(1)} all-to-all(bf16[16,16,768]{2,1,0:T(8,128)(2,1)S(1)} %get-tuple-element.16), channel_id=1, replica_groups=mesh['kv_0'=4,'kv_1'=4,'tp'=16] {'kv_0','kv_1'}, dimensions={0} | all-to-all | bytes 786432 | tf_op jit(solution)/shard_map/all_to_all | solution.py:26
  83.7 0.0 copy-done.7
  83.7 0.3 shard_map.189
  84.0 11.8 %all_to_all.41.got_ref = bf16[16,16,128]{2,1,0:T(8,128)(2,1)S(1)} all-to-all(bf16[16,16,128]{2,1,0:T(8,128)(2,1)S(1)} %shard_map.189), channel_id=1, replica_groups=mesh['kv_0'=4,'kv_1'=4,'tp'=16] {'tp'}, dimensions={0} | all-to-all | bytes 131072 | tf_op jit(solution)/shard_map/all_to_all | solution.py:26
  95.8 0.6 shard_map.190
  (1 shorter events, 0.0 us)
Async XLA Ops:
  0.0 0.8 copy-start.13
  0.0 0.9 copy-start.12
  0.0 0.9 copy-start.3
  0.0 1.0 copy-start.2
  0.0 0.9 copy-start.14
  1.0 16.8 %copy-start.4 = (bf16[352,128]{1,0:T(8,128)(2,1)S(1)}, bf16[352,128]{1,0:T(8,128)(2,1)}, u32[]{:S(2)}) copy-start(bf16[352,128]{1,0:T(8,128)(2,1)} %down_ref.2) | copy-start | bytes 270340
  17.8 18.2 %copy-start.8 = (bf16[128,128]{1,0:T(8,128)(2,1)S(1)}, bf16[128,128]{1,0:T(8,128)(2,1)}, u32[]{:S(2)}) copy-start(bf16[128,128]{1,0:T(8,128)(2,1)} %wq_ref.1) | copy-start | bytes 98308
  17.8 18.2 %copy-start.9 = (bf16[128,128]{1,0:T(8,128)(2,1)S(1)}, bf16[128,128]{1,0:T(8,128)(2,1)}, u32[]{:S(2)}) copy-start(bf16[128,128]{1,0:T(8,128)(2,1)} %wk_ref.1) | copy-start | bytes 98308
  17.8 18.2 %copy-start.10 = (bf16[128,128]{1,0:T(8,128)(2,1)S(1)}, bf16[128,128]{1,0:T(8,128)(2,1)}, u32[]{:S(2)}) copy-start(bf16[128,128]{1,0:T(8,128)(2,1)} %wv_ref.1) | copy-start | bytes 98308
  17.8 18.2 %copy-start.15 = (bf16[128]{0:T(256)(128)(2,1)S(1)}, bf16[128]{0:T(256)(128)(2,1)}, u32[]{:S(2)}) copy-start(bf16[128]{0:T(256)(128)(2,1)} %param.25) | copy-start | bytes 772
  36.0 9.8 %copy-start = (bf16[16,1024,1,128]{3,1,2,0:T(8,128)(2,1)S(1)}, bf16[16,1024,1,128]{3,1,2,0:T(8,128)(2,1)}, u32[]{:S(2)}) copy-start(bf16[16,1024,1,128]{3,1,2,0:T(8,128)(2,1)} %param.21) | copy-start | bytes 12582916
  36.0 9.8 %copy-start.1 = (bf16[16,1024,1,128]{3,1,2,0:T(8,128)(2,1)S(1)}, bf16[16,1024,1,128]{3,1,2,0:T(8,128)(2,1)}, u32[]{:S(2)}) copy-start(bf16[16,1024,1,128]{3,1,2,0:T(8,128)(2,1)} %param.22) | copy-start | bytes 12582916
  45.8 12.1 %copy-start.11 = (bf16[128,128]{1,0:T(8,128)(2,1)S(1)}, bf16[128,128]{1,0:T(8,128)(2,1)}, u32[]{:S(2)}) copy-start(bf16[128,128]{1,0:T(8,128)(2,1)} %w_ref.1) | copy-start | bytes 98308
  45.8 12.1 %copy-start.16 = (bf16[128]{0:T(256)(128)(2,1)S(1)}, bf16[128]{0:T(256)(128)(2,1)}, u32[]{:S(2)}) copy-start(bf16[128]{0:T(256)(128)(2,1)} %param.24) | copy-start | bytes 772
  58.0 13.3 %copy-start.5 = (bf16[128,352]{0,1:T(8,128)(2,1)S(1)}, bf16[128,352]{0,1:T(8,128)(2,1)}, u32[]{:S(2)}) copy-start(bf16[128,352]{0,1:T(8,128)(2,1)} %param.35) | copy-start | bytes 270340
  58.0 13.3 %copy-start.6 = (bf16[128,352]{0,1:T(8,128)(2,1)S(1)}, bf16[128,352]{0,1:T(8,128)(2,1)}, u32[]{:S(2)}) copy-start(bf16[128,352]{0,1:T(8,128)(2,1)} %param.36) | copy-start | bytes 270340
  58.0 13.2 %copy-start.17 = (bf16[128]{0:T(256)(128)(2,1)S(1)}, bf16[128]{0:T(256)(128)(2,1)}, u32[]{:S(2)}) copy-start(bf16[128]{0:T(256)(128)(2,1)} %param.34) | copy-start | bytes 772
  71.2 12.4 %copy-start.7 = (bf16[352,128]{1,0:T(8,128)(2,1)S(1)}, bf16[352,128]{1,0:T(8,128)(2,1)}, u32[]{:S(2)}) copy-start(bf16[352,128]{1,0:T(8,128)(2,1)} %down_ref.3) | copy-start | bytes 270340

commit v4 on v3

--- a/solution.py
+++ b/solution.py
@@ -13,11 +13,14 @@
 DK = 64
 DV = 128
 SEQS = 16
-KV = ("kv_0", "kv_1")
+KV = ("kv_0", "kv_a", "kv_b")
+HALF = ("kv_0", "kv_b")
+PAIR = [(x, 3 - x) for x in range(4)]
 EPSILON = 1e-06
 ROTARY_BASE = 10000.0
 OUTPUT_KEEP = 0.8
 MASKED_SCORE = -1e30
+GATE, UP, W_OUT, TOKENS, GAINS, PACK = 384, 736, 1088, 1216, 1232, 1264
 F32 = jnp.float32
 BF16 = jnp.bfloat16
 
@@ -81,14 +84,12 @@
     return out
 
 
-def gate_up_products(stream_f, gain_ref, gate_ref, up_ref, out_ref):
-    scaled = (stream_f * gain_ref[...].astype(F32)).astype(BF16)
-    square = jnp.sum(stream_f * stream_f, axis=1, keepdims=True)
-    gate = dot_rows(scaled, gate_ref[...]).astype(BF16)
-    up = dot_rows(scaled, up_ref[...]).astype(BF16)
-    put_copies(out_ref, 0, gate)
+def gate_up_products(streams, gains, gates, ups, out_ref):
+    scaled = [(x * g.astype(F32)).astype(BF16) for x, g in zip(streams, gains)]
+    square = sum(jnp.sum(x * x, axis=1, keepdims=True) for x in streams)
+    put_copies(out_ref, 0, sum(map(dot_rows, scaled, gates)).astype(BF16))
     put_copies(out_ref, 352, with_columns(32, pieces(square, 2)))
-    put_copies(out_ref, 384, up)
+    put_copies(out_ref, 384, sum(map(dot_rows, scaled, ups)).astype(BF16))
     put_copies(out_ref, 736, jnp.zeros((SEQS, 32), BF16))
 
 
@@ -117,43 +118,87 @@
 
 
 def first_products(tokens_ref, gain_ref, gate_ref, up_ref, side_ref, out_ref):
-    gate_up_products(tokens_ref[...].astype(F32), gain_ref, gate_ref, up_ref, out_ref)
-
-
-def second_products(stream_ref, got_ref, gain_ref, gate_ref, up_ref, out_ref, second_ref):
+    gate_up_products(
+        [tokens_ref[...].astype(F32)], [gain_ref[...]], [gate_ref[...]], [up_ref[...]], out_ref
+    )
+
+
+def second_products(stream_ref, got_ref, gain_ref, gate_ref, up_ref, pack_ref, out_ref, second_ref):
     second = (stream_ref[...].astype(F32) + total(got_ref)).astype(BF16)
-    second_ref[...] = second
-    gate_up_products(second.astype(F32), gain_ref, gate_ref, up_ref, out_ref)
-
-
-def down_products(got_ref, down_ref, out_ref):
+    second_ref[...] = second[:, :128]
+    second = second.astype(F32)
+    gate_up_products(
+        [second[:, :128], second[:, 128:]],
+        [gain_ref[...], pack_ref[GAINS + 16 : GAINS + 17]],
+        [gate_ref[...], pack_ref[GATE : GATE + 352]],
+        [up_ref[...], pack_ref[UP : UP + 352]],
+        out_ref,
+    )
+
+
+def hidden_units(got_ref):
     summed = total(got_ref)
     square = summed[:, 352:353] + summed[:, 353:354]
     row_scale = lax.rsqrt(square / D + EPSILON)
     gate = row_scale * summed[:, :352]
     up = row_scale * summed[:, 384:736]
-    hidden = (gate / (1.0 + jnp.exp(-gate)) * up).astype(BF16)
+    return (gate / (1.0 + jnp.exp(-gate)) * up).astype(BF16)
+
+
+def hidden_and_pack(
+    got_ref, wq_ref, wk_ref, wv_ref, gate_ref, up_ref, w_out_ref, tokens_ref, attn_gain_ref,
+    second_gain_ref, hidden_ref, pack_ref
+):
+    hidden_ref[...] = hidden_units(got_ref)
+    at = 0
+    for ref in (wq_ref, wk_ref, wv_ref, gate_ref, up_ref, w_out_ref, tokens_ref):
+        pack_ref[at : at + ref.shape[0], :] = ref[...]
+        at += ref.shape[0]
+    for ref in (attn_gain_ref, second_gain_ref):
+        pack_ref[at : at + 16, :] = jnp.broadcast_to(ref[...], (16, 128))
+        at += 16
+
+
+def down_products_of_pair(hidden_ref, down_ref, other_ref, out_ref):
+    hidden = hidden_ref[...]
     put_copies(out_ref, 0, dot(hidden, down_ref[...]).astype(BF16))
-
-
-def head_products(tokens_ref, got_ref, gain_ref, wq_ref, wk_ref, wv_ref, out_ref, first_ref):
-    first = (tokens_ref[...].astype(F32) + 0.5 * total(got_ref)).astype(BF16)
+    put_copies(out_ref, 128, dot(hidden, other_ref[...]).astype(BF16))
+
+
+def down_products(got_ref, down_ref, out_ref):
+    put_copies(out_ref, 0, dot(hidden_units(got_ref), down_ref[...]).astype(BF16))
+
+
+def head_products(
+    tokens_ref, got_ref, gain_ref, wq_ref, wk_ref, wv_ref, pack_ref, out_ref, first_ref
+):
+    tokens = jnp.concatenate([tokens_ref[...], pack_ref[TOKENS : TOKENS + 16]], axis=1)
+    first = (tokens.astype(F32) + 0.5 * total(got_ref)).astype(BF16)
     first_ref[...] = first
     stream_f = first.astype(F32)
-    scaled = (stream_f * gain_ref[...].astype(F32)).astype(BF16)
     square = jnp.sum(stream_f * stream_f, axis=1, keepdims=True)
-    query = dot(scaled, wq_ref[...]).astype(BF16)
-    key = dot(scaled, wk_ref[...])
-    value = dot(scaled, wv_ref[...])
+    own = (stream_f[:, :128] * gain_ref[...].astype(F32)).astype(BF16)
+    other = (stream_f[:, 128:] * pack_ref[GAINS : GAINS + 1].astype(F32)).astype(BF16)
+    query, key, value = (
+        dot(own, ref[...]) + dot(other, pack_ref[128 * i : 128 * i + 128])
+        for i, ref in enumerate((wq_ref, wk_ref, wv_ref))
+    )
+    query = query.astype(BF16)
     diagonal = lax.broadcasted_iota(jnp.int32, (SEQS, 128), 0) == lax.broadcasted_iota(
         jnp.int32, (SEQS, 128), 1
     )
     high, rest = pieces(jnp.sum(jnp.where(diagonal, square, 0.0), axis=0, keepdims=True), 2)
     row = lax.broadcasted_iota(jnp.int32, (8, 128), 0)
     squares = jnp.where(row == 2, high.astype(F32), jnp.where(row == 3, rest.astype(F32), 0.0))
-    for j in range(SEQS):
+    near = lax.axis_index("kv_a") == 0
+
+    def row_of(x, peer):
+        at = 4 * (peer // 2) + peer % 2
+        return jnp.where(near, x[at : at + 1], x[at + 2 : at + 3])
+
+    for j in range(out_ref.shape[0]):
         out_ref[j, :SEQS, :] = query
-        tail = jnp.where(row == 0, key[j : j + 1], jnp.where(row == 1, value[j : j + 1], squares))
+        tail = jnp.where(row == 0, row_of(key, j), jnp.where(row == 1, row_of(value, j), squares))
         out_ref[j, SEQS:, :] = tail.astype(BF16)
 
 
@@ -233,7 +278,7 @@
         out_ref[j, rows:, :] = stats
 
 
-def out_products(got_ref, side_ref, gain_ref, w_ref, out_ref):
+def out_products(got_ref, side_ref, gain_ref, w_ref, pack_ref, out_ref):
     count = got_ref.shape[0]
     rows = 2 * SEQS
     stats = [got_ref[j, rows:, :].astype(F32) for j in range(count)]
@@ -253,6 +298,7 @@
     norm_scale = lax.rsqrt(jnp.mean(head * head, axis=1, keepdims=True) + EPSILON)
     normed = (head * norm_scale * gain_ref[...].astype(F32) * OUTPUT_KEEP).astype(BF16)
     put_copies(out_ref, 0, dot(normed, w_ref[...]).astype(BF16))
+    put_copies(out_ref, 128, dot(normed, pack_ref[W_OUT : W_OUT + 128]).astype(BF16))
 
 
 def last_sum(stream_ref, got_ref, out_ref):
@@ -268,44 +314,58 @@
     values = cache_values.reshape(SEQS, -1, DV)
     row = lambda g: g.reshape(1, -1)
     shape = jax.ShapeDtypeStruct
-    wide = shape((16, SEQS, 768), BF16)
+
+    def from_partner(x):
+        return lax.ppermute(x, ("kv_a", "kv_b"), PAIR)
+
     narrow = shape((16, SEQS, 128), BF16)
+    double = shape((16, SEQS, 256), BF16)
     stream = shape((SEQS, 128), BF16)
 
+    other_down = from_partner(first_down)
     steps = local_call(rotary_steps, shape((SEQS, 128), F32))
     side, limit = local_call(
         side_tables, (shape((3, SEQS, 128), F32), shape((2 * SEQS, 128), jnp.int32)),
         lambdas, row(lengths), steps, scalars=1, micros=0.01,
     )
     sent = local_call(
-        first_products, wide, tokens, row(first_gain), first_gate.T, first_up.T, side
-    )
-    sent = local_call(down_products, narrow, exchange(sent, KV), first_down)
+        first_products, shape((16, SEQS, 768), BF16),
+        tokens, row(first_gain), first_gate.T, first_up.T, side,
+    )
+    got = exchange(sent, KV)
+    hidden, pack = local_call(
+        hidden_and_pack, (shape((SEQS, 352), BF16), shape((PACK, 128), BF16)),
+        got, w_query, w_key, w_value, second_gate.T, second_up.T, w_out, tokens,
+        row(attn_gain), row(second_gain),
+    )
+    pack = from_partner(pack)
+    sent = local_call(down_products_of_pair, double, hidden, first_down, other_down)
     sent, first = local_call(
-        head_products, (shape((16, SEQS + 8, 128), BF16), stream),
-        tokens, exchange(sent, "tp"), row(attn_gain), w_query, w_key, w_value,
+        head_products, (shape((8, SEQS + 8, 128), BF16), shape((SEQS, 256), BF16)),
+        tokens, exchange(sent, "tp"), row(attn_gain), w_query, w_key, w_value, pack,
     )
     sent = local_call(
         attention, shape((16, 2 * SEQS + 8, 128), BF16),
-        exchange(sent, KV), side, limit, keys, values,
+        exchange(sent, HALF), side, limit, keys, values,
     )
     sent = local_call(
-        out_products, narrow, exchange(sent, KV), side, row(head_gain), w_out
+        out_products, double, exchange(sent, KV), side, row(head_gain), w_out, pack
     )
     sent, second = local_call(
-        second_products, (wide, stream),
-        first, exchange(sent, "tp"), row(second_gain), second_gate.T, second_up.T,
-    )
-    sent = local_call(down_products, narrow, exchange(sent, KV), second_down)
+        second_products, (shape((8, SEQS, 768), BF16), stream),
+        first, exchange(sent, "tp"), row(second_gain), second_gate.T, second_up.T, pack,
+    )
+    sent = local_call(down_products, narrow, exchange(sent, HALF), second_down)
     return local_call(last_sum, stream, second, exchange(sent, "tp"))
 
 
 def solution(mesh):
-    finer = Mesh(mesh.devices.reshape(4, 4, mesh.shape["tp"]), ("kv_0", "kv_1", "tp"))
+    finer = Mesh(mesh.devices.reshape(4, 2, 2, mesh.shape["tp"]), (*KV, "tp"))
     cache = P(None, KV, "tp", None)
     placed = (
         P(None, KV), P(), cache, cache, P("tp"), P(), P(KV), P(KV, "tp"), P(KV, "tp"),
         P(KV, "tp"), P("tp", KV), P(KV), P(KV, "tp"), P(KV, "tp"), P("tp", KV), P(KV),
         P(KV, "tp"), P(KV, "tp"), P("tp", KV),
     )
+
     return jax.shard_map(local, mesh=finer, in_specs=placed, out_specs=P(None, KV), check_vma=False)

time: 96.8 us -> 97.2 us (level)
  blocking collectives: 91.1 us -> 73.6 us
  starting transfers between devices: 0 us -> 10.3 us
  waiting for transfers between devices: 0 us -> 6.57 us
    all_to_all x7 -> x6, blocking collectives: 91.1 us -> 73.6 us  [exchange(): return lax.all_to_all(copies, axis, split_axis=0, concat_axis=0, tiled=True)]
    all_to_all x0 -> x1, starting transfers between devices: none -> 7.57 us  [exchange(): return lax.all_to_all(copies, axis, split_axis=0, concat_axis=0, tiled=True)]
    all_to_all x0 -> x1, waiting for transfers between devices: none -> 6.56 us  [exchange(): return lax.all_to_all(copies, axis, split_axis=0, concat_axis=0, tiled=True)]
    ppermute x0 -> x2, starting transfers between devices: none -> 2.75 us  [from_partner(): return lax.ppermute(x, ('kv_a', 'kv_b'), PAIR)]
    pallas_call x10 -> x11, Pallas kernels: 4.3 us -> 5.15 us  [local_call(): pl.pallas_call(body, out_shape=outs, in_specs=[pl.BlockSpec(memory_space=...]
  transfers between devices with their start and end apart: 0 -> 3, of which waited for: 0 -> 1; matrix products, arithmetic and copies ran while one was open for 0% -> 0% of each run, Pallas kernels for 0% -> 0%
where the time goes in v4:
time: 97.2 us; the launch traced here: 96.8 us
  blocking collectives  73.6 us (76%)
  starting transfers between devices  10.3 us (11%)
  waiting for transfers between devices  6.57 us (7%)
  Pallas kernels  5.15 us (5%)
  between operations  1 us (1%)
    all_to_all x6, blocking collectives, exchange(): return lax.all_to_all(copies, axis, split_axis=0, concat_axis=0, tiled=True)  73.6 us
    all_to_all x1, starting transfers between devices, exchange(): return lax.all_to_all(copies, axis, split_axis=0, concat_axis=0, tiled=True)  7.57 us
    all_to_all x1, waiting for transfers between devices, exchange(): return lax.all_to_all(copies, axis, split_axis=0, concat_axis=0, tiled=True)  6.56 us
    pallas_call x11, Pallas kernels, local_call(): pl.pallas_call(body, out_shape=outs, in_specs=[pl.BlockSpec(memory_space=...  5.15 us
    ppermute x2, starting transfers between devices, from_partner(): return lax.ppermute(x, ('kv_a', 'kv_b'), PAIR)  2.75 us
  transfers between devices with their start and end apart: 3, of which 1 were waited for; matrix products, arithmetic and copies ran while one was open for 0% of the time, Pallas kernels for 0%

profile of v4, /device:TPU:1, one launch (start us, length us, event | category | flops | bytes accessed | tf_op | source)
XLA Modules:
  0.0 96.8 jit_solution(17852406291284566977)
XLA Ops:
  0.0 0.0 copy-start.13
  0.0 0.0 copy-start.14
  0.0 0.0 copy-start.2
  0.0 0.0 copy-start.3
  0.0 0.0 copy-start.12
  0.8 0.0 copy-done.13
  0.8 0.1 shard_map.182
  0.9 0.0 copy-done.14
  0.9 0.0 copy-done.2
  0.9 0.0 copy-done.3
  1.0 0.0 copy-done.12
  1.0 0.0 copy-start.4
  1.0 0.0 copy-start.5
  1.0 0.0 copy-start.6
  1.0 0.0 copy-start.8
  1.0 0.0 copy-start.9
  1.0 0.0 copy-start.10
  1.0 0.0 copy-start.11
  1.1 0.0 copy-start.15
  1.1 0.0 copy-start.17
  1.1 0.9 shard_map.183
  2.0 7.6 %all-to-all-start = ((bf16[16,16,768]{2,1,0:T(8,128)(2,1)}), bf16[16,16,768]{2,1,0:T(8,128)(2,1)S(1)}, u32[]{:S(2)}, u32[]{:S(2)}) async-start(bf16[16,16,768]{2,1,0:T(8,128)(2,1)} %shard_map.183), calls=%async_computation | async-start | bytes 786432 | tf_op jit(solution)/shard_map/all_to_all | solution.py:29
  9.6 0.0 copy-done.4
  9.6 2.7 %collective-permute-start = (bf16[352,128]{1,0:T(8,128)(2,1)S(1)}, bf16[352,128]{1,0:T(8,128)(2,1)S(1)}, u32[]{:S(2)}, u32[]{:S(2)}) collective-permute-start(bf16[352,128]{1,0:T(8,128)(2,1)S(1)} %copy-done.4), channel_id=1, source_target_pairs={{0,48},{16,32},{32,16},{48,0},{1,49},{17,33},{33,17},{49,1},{2,50}... | collective-permute-start | bytes 270344 | tf_op jit(solution)/shard_map/ppermute | solution.py:319
  12.3 6.6 %all-to-all-done.got_ref = bf16[16,16,768]{2,1,0:T(8,128)(2,1)S(1)} async-done(((bf16[16,16,768]{2,1,0:T(8,128)(2,1)}), bf16[16,16,768]{2,1,0:T(8,128)(2,1)S(1)}, u32[]{:S(2)}, u32[]{:S(2)}) %all-to-all-start) | async-done | bytes 393248 | tf_op jit(solution)/shard_map/all_to_all | solution.py:29
  18.8 0.0 copy-done.5
  18.8 0.0 copy-done.6
  18.8 0.0 copy-done.8
  18.8 0.0 copy-done.9
  18.9 0.0 copy-done.10
  18.9 0.0 copy-done.11
  18.9 0.0 copy-done.15
  18.9 0.0 copy-done.17
  18.9 0.2 shard_map.184
  19.1 0.1 collective-permute-start.1
  19.2 0.0 collective-permute-done.other_ref
  19.2 0.2 shard_map.185
  19.4 19.5 %all_to_all.35.got_ref = bf16[16,16,256]{2,1,0:T(8,128)(2,1)S(1)} all-to-all(bf16[16,16,256]{2,1,0:T(8,128)(2,1)S(1)} %shard_map.185), channel_id=1, replica_groups=mesh['kv_0'=4,'kv_a'=2,'kv_b'=2,'tp'=16] {'tp'}, dimensions={0} | all-to-all | bytes 262144 | tf_op jit(solution)/shard_map/all_to_all | solution.py:29
  38.9 0.0 copy-start
  38.9 0.0 copy-start.1
  38.9 0.0 collective-permute-done.1.pack_ref
  38.9 0.2 shard_map.186
  39.1 7.9 %all_to_all.36.got_ref = bf16[8,24,128]{2,1,0:T(8,128)(2,1)S(1)} all-to-all(bf16[8,24,128]{2,1,0:T(8,128)(2,1)S(1)} %get-tuple-element.17), channel_id=1, replica_groups=mesh['kv_0'=4,'kv_a'=2,'kv_b'=2,'tp'=16] {'kv_0','kv_b'}, dimensions={0} | all-to-all | bytes 98304 | tf_op jit(solution)/shard_map/all_to_all | solution.py:29
  47.0 0.0 copy-done
  47.0 0.0 copy-done.1
  47.0 0.0 copy-start.16
  47.0 1.9 %shard_map.187 = bf16[16,40,128]{2,1,0:T(8,128)(2,1)S(1)} custom-call(bf16[8,24,128]{2,1,0:T(8,128)(2,1)S(1)} %all_to_all.36.got_ref, f32[3,16,128]{2,1,0:T(8,128)S(1)} %get-tuple-element.13.side_ref, s32[32,128]{1,0:T(8,128)S(1)} %get-tuple-element.18.limit_ref, bf16[16,1024,128]{2,1,0:T(8,128)(2,1)S(1)} %bitcast.11, bf16[16,1024,128]{2,1,0:T(8,128)(2,1)S(1)} %bitcast.12), custom_call_target="tpu_custom_call" | custom-call | flops 5000000000 | bytes 65536 | tf_op jit(solution)/shard_map/pallas_call | solution.py:37
  48.9 11.9 %all_to_all.37.got_ref = bf16[16,40,128]{2,1,0:T(8,128)(2,1)S(1)} all-to-all(bf16[16,40,128]{2,1,0:T(8,128)(2,1)S(1)} %shard_map.187), channel_id=1, replica_groups=mesh['kv_0'=4,'kv_a'=2,'kv_b'=2,'tp'=16] {'kv_0','kv_a','kv_b'}, dimensions={0} | all-to-all | bytes 327680 | tf_op jit(solution)/shard_map/all_to_all | solution.py:29
  60.8 0.0 copy-done.16
  60.8 0.5 shard_map.188
  61.3 14.1 %all_to_all.38.got_ref = bf16[16,16,256]{2,1,0:T(8,128)(2,1)S(1)} all-to-all(bf16[16,16,256]{2,1,0:T(8,128)(2,1)S(1)} %shard_map.188), channel_id=1, replica_groups=mesh['kv_0'=4,'kv_a'=2,'kv_b'=2,'tp'=16] {'tp'}, dimensions={0} | all-to-all | bytes 262144 | tf_op jit(solution)/shard_map/all_to_all | solution.py:29
  75.5 0.0 copy-start.7
  75.5 0.2 shard_map.189
  75.7 9.1 %all_to_all.39.got_ref = bf16[8,16,768]{2,1,0:T(8,128)(2,1)S(1)} all-to-all(bf16[8,16,768]{2,1,0:T(8,128)(2,1)S(1)} %get-tuple-element.20), channel_id=1, replica_groups=mesh['kv_0'=4,'kv_a'=2,'kv_b'=2,'tp'=16] {'kv_0','kv_b'}, dimensions={0} | all-to-all | bytes 393216 | tf_op jit(solution)/shard_map/all_to_all | solution.py:29
  84.8 0.0 copy-done.7
  84.8 0.3 shard_map.190
  85.1 11.1 %all_to_all.40.got_ref = bf16[16,16,128]{2,1,0:T(8,128)(2,1)S(1)} all-to-all(bf16[16,16,128]{2,1,0:T(8,128)(2,1)S(1)} %shard_map.190), channel_id=1, replica_groups=mesh['kv_0'=4,'kv_a'=2,'kv_b'=2,'tp'=16] {'tp'}, dimensions={0} | all-to-all | bytes 131072 | tf_op jit(solution)/shard_map/all_to_all | solution.py:29
  96.2 0.6 shard_map.191
  (1 shorter events, 0.0 us)
Async XLA Ops:
  0.0 0.8 copy-start.13
  0.0 0.9 copy-start.14
  0.0 0.9 copy-start.2
  0.0 1.0 copy-start.3
  0.0 0.9 copy-start.12
  1.0 8.6 %copy-start.4 = (bf16[352,128]{1,0:T(8,128)(2,1)S(1)}, bf16[352,128]{1,0:T(8,128)(2,1)}, u32[]{:S(2)}) copy-start(bf16[352,128]{1,0:T(8,128)(2,1)} %down_ref.2) | copy-start | bytes 270340
  1.0 17.9 %copy-start.5 = (bf16[128,352]{0,1:T(8,128)(2,1)S(1)}, bf16[128,352]{0,1:T(8,128)(2,1)}, u32[]{:S(2)}) copy-start(bf16[128,352]{0,1:T(8,128)(2,1)} %param.35) | copy-start | bytes 270340
  1.0 17.8 %copy-start.6 = (bf16[128,352]{0,1:T(8,128)(2,1)S(1)}, bf16[128,352]{0,1:T(8,128)(2,1)}, u32[]{:S(2)}) copy-start(bf16[128,352]{0,1:T(8,128)(2,1)} %param.36) | copy-start | bytes 270340
  1.0 17.8 %copy-start.8 = (bf16[128,128]{1,0:T(8,128)(2,1)S(1)}, bf16[128,128]{1,0:T(8,128)(2,1)}, u32[]{:S(2)}) copy-start(bf16[128,128]{1,0:T(8,128)(2,1)} %wq_ref.3) | copy-start | bytes 98308
  1.0 17.8 %copy-start.9 = (bf16[128,128]{1,0:T(8,128)(2,1)S(1)}, bf16[128,128]{1,0:T(8,128)(2,1)}, u32[]{:S(2)}) copy-start(bf16[128,128]{1,0:T(8,128)(2,1)} %wk_ref.3) | copy-start | bytes 98308
  1.0 17.8 %copy-start.10 = (bf16[128,128]{1,0:T(8,128)(2,1)S(1)}, bf16[128,128]{1,0:T(8,128)(2,1)}, u32[]{:S(2)}) copy-start(bf16[128,128]{1,0:T(8,128)(2,1)} %wv_ref.3) | copy-start | bytes 98308
  1.0 17.8 %copy-start.11 = (bf16[128,128]{1,0:T(8,128)(2,1)S(1)}, bf16[128,128]{1,0:T(8,128)(2,1)}, u32[]{:S(2)}) copy-start(bf16[128,128]{1,0:T(8,128)(2,1)} %w_ref.1) | copy-start | bytes 98308
  1.1 17.8 %copy-start.15 = (bf16[128]{0:T(256)(128)(2,1)S(1)}, bf16[128]{0:T(256)(128)(2,1)}, u32[]{:S(2)}) copy-start(bf16[128]{0:T(256)(128)(2,1)} %param.25) | copy-start | bytes 772
  1.1 17.8 %copy-start.17 = (bf16[128]{0:T(256)(128)(2,1)S(1)}, bf16[128]{0:T(256)(128)(2,1)}, u32[]{:S(2)}) copy-start(bf16[128]{0:T(256)(128)(2,1)} %param.34) | copy-start | bytes 772
  2.0 16.8 %all-to-all-start = ((bf16[16,16,768]{2,1,0:T(8,128)(2,1)}), bf16[16,16,768]{2,1,0:T(8,128)(2,1)S(1)}, u32[]{:S(2)}, u32[]{:S(2)}) async-start(bf16[16,16,768]{2,1,0:T(8,128)(2,1)} %shard_map.183), calls=%async_computation | async-start | bytes 786432 | tf_op jit(solution)/shard_map/all_to_all | solution.py:29
  9.6 9.6 %collective-permute-start = (bf16[352,128]{1,0:T(8,128)(2,1)S(1)}, bf16[352,128]{1,0:T(8,128)(2,1)S(1)}, u32[]{:S(2)}, u32[]{:S(2)}) collective-permute-start(bf16[352,128]{1,0:T(8,128)(2,1)S(1)} %copy-done.4), channel_id=1, source_target_pairs={{0,48},{16,32},{32,16},{48,0},{1,49},{17,33},{33,17},{49,1},{2,50}... | collective-permute-start | bytes 270344 | tf_op jit(solution)/shard_map/ppermute | solution.py:319
  19.1 19.8 %collective-permute-start.1 = (bf16[1264,128]{1,0:T(8,128)(2,1)S(1)}, bf16[1264,128]{1,0:T(8,128)(2,1)S(1)}, u32[]{:S(2)}, u32[]{:S(2)}) collective-permute-start(bf16[1264,128]{1,0:T(8,128)(2,1)S(1)} %get-tuple-element.15), channel_id=1, source_target_pairs={{0,48},{16,32},{32,16},{48,0},{1,49},{17,33},{33,17},{49,1},{2,50}... | collective-permute-start | bytes 970760 | tf_op jit(solution)/shard_map/ppermute | solution.py:319
  38.9 8.1 %copy-start = (bf16[16,1024,1,128]{3,1,2,0:T(8,128)(2,1)S(1)}, bf16[16,1024,1,128]{3,1,2,0:T(8,128)(2,1)}, u32[]{:S(2)}) copy-start(bf16[16,1024,1,128]{3,1,2,0:T(8,128)(2,1)} %param.21) | copy-start | bytes 12582916
  38.9 8.1 %copy-start.1 = (bf16[16,1024,1,128]{3,1,2,0:T(8,128)(2,1)S(1)}, bf16[16,1024,1,128]{3,1,2,0:T(8,128)(2,1)}, u32[]{:S(2)}) copy-start(bf16[16,1024,1,128]{3,1,2,0:T(8,128)(2,1)} %param.22) | copy-start | bytes 12582916
  47.0 13.8 %copy-start.16 = (bf16[128]{0:T(256)(128)(2,1)S(1)}, bf16[128]{0:T(256)(128)(2,1)}, u32[]{:S(2)}) copy-start(bf16[128]{0:T(256)(128)(2,1)} %param.24) | copy-start | bytes 772
  75.5 9.3 %copy-start.7 = (bf16[352,128]{1,0:T(8,128)(2,1)S(1)}, bf16[352,128]{1,0:T(8,128)(2,1)}, u32[]{:S(2)}) copy-start(bf16[352,128]{1,0:T(8,128)(2,1)} %down_ref.3) | copy-start | bytes 270340
